TPU v7x, 32 devices: a whole 2x2x4 slice. The times are simulated.
32 devices in a mesh: rep: 2 (over x), fs: 8 (over z, y), tp: 2 (over core).
Axes of the slice: x: 2, y: 2, z: 4, core: 2. Of those that a mesh axis runs over, the one named last changes fastest.
Arguments:
- tokens: bfloat16 [8192, 2048], P(('rep', 'fs')), may hold values from -6 to 6
- mixer_gain: float32 [2048], replicated, may hold values from 0.1 to 1.9
- pool_input: float32 [2048, 1024], P('fs', 'tp'), may hold values from -0.125 to 0.125
- input_scale: float32 [1024], P('tp'), may hold values from 0.5 to 2
- group_mix: float32 [128, 1024], P(None, 'tp'), may hold values from -0.5 to 0.5
- group_scale: float32 [1024], P('tp'), may hold values from 0.5 to 2
- pool_output: float32 [2048, 1024], P('fs', 'tp'), may hold values from -0.1875 to 0.1875
- output_scale: float32 [2048], P('fs'), may hold values from 0.5 to 2
- channel_gain: float32 [2048], replicated, may hold values from 0.1 to 1.9
- gate_weight: float32 [2048, 5632], P('fs', 'tp'), may hold values from -0.125 to 0.125
- gate_scale: float32 [5632], P('tp'), may hold values from 0.5 to 2
- up_weight: float32 [2048, 5632], P('fs', 'tp'), may hold values from -0.125 to 0.125
- up_scale: float32 [5632], P('tp'), may hold values from 0.5 to 2
- down_weight: float32 [2048, 5632], P('fs', 'tp'), may hold values from -0.078125 to 0.078125
- down_scale: float32 [2048], P('fs'), may hold values from 0.5 to 2
Outputs:
- layer_out: bfloat16 [8192, 2048], P(('rep', 'fs'))
All inputs are finite; a program needn't handle non-finite values.
Results may differ from a plain program's by a relative error of at most 0.02.
Values may be sent and summed in bfloat16 or wider, within the bound.
No kernel may reach another device: no remote copies, remote signals or barrier semaphores. Data moves between devices by JAX's collectives and lax.ppermute only.
A program may use at most 128 MiB of HBM per device.

v0:
```python
import functools
import jax
import jax.numpy as jnp
from jax import lax
from jax.experimental import pallas as pl
from jax.experimental.pallas import tpu as pltpu
from jax.sharding import PartitionSpec as P


POOL_GROUP = 256
BF = jnp.bfloat16
F32 = jnp.float32
epsilon = 1e-06


def rms_norm(row_block, gain_row):
    floats = row_block.astype(F32)
    scaled = floats * lax.rsqrt(jnp.mean(floats * floats, axis=-1, keepdims=True) + epsilon)
    return (scaled * gain_row).astype(BF)


def transposed_product(left_rows, weight_rows):
    return lax.dot_general(
        left_rows, weight_rows, (((1,), (1,)), ((), ())), preferred_element_type=F32
    )


def plain_body(
    tokens, mixer_gain, pool_input, input_scale, group_mix, group_scale, pool_output, output_scale,
    channel_gain, gate_weight, gate_scale, up_weight, up_scale, down_weight, down_scale,
):
    def gather(value):
        return lax.all_gather(value, "fs", axis=0, tiled=True)

    length = tokens.shape[0]
    block_width, local_width = group_mix.shape
    normed = rms_norm(tokens, mixer_gain)
    input_full = gather(pool_input.astype(BF))
    output_full = gather(pool_output.astype(BF))
    output_feature, down_feature = gather(output_scale), gather(down_scale)
    pool_in = (jnp.dot(normed, input_full, preferred_element_type=F32) * input_scale).astype(BF)
    places = jnp.arange(length, dtype=jnp.int32)
    offsets = places[:, None] - places[None, :]
    chunk = min(POOL_GROUP, local_width)
    pieces = []
    for piece in range(local_width // chunk):
        group_index = (lax.axis_index("tp") * local_width + piece * chunk) // POOL_GROUP
        window = lax.shift_left(jnp.int32(2), group_index.astype(jnp.int32))
        band_mask = ((offsets >= 0) & (offsets < window)).astype(BF)
        columns = pool_in[:, piece * chunk : (piece + 1) * chunk]
        window_sums = jnp.dot(band_mask, columns, preferred_element_type=F32)
        counts = jnp.minimum(places + 1, window).astype(F32)
        pieces.append((window_sums / counts[:, None] - columns.astype(F32)).astype(BF))
    pooled = jnp.concatenate(pieces, axis=1)
    local_blocks = local_width // block_width
    mixed_raw = jnp.einsum(
        "sgc,cgd->sgd",
        pooled.reshape(length, local_blocks, block_width),
        group_mix.astype(BF).reshape(block_width, local_blocks, block_width),
        preferred_element_type=F32,
    ).reshape(length, local_width)
    grouped = (mixed_raw * group_scale).astype(BF)
    partial_value = (transposed_product(grouped, output_full) * output_feature).astype(BF)
    mixer_out = lax.psum(partial_value, "tp").astype(F32)
    middle = (tokens.astype(F32) + mixer_out).astype(BF)
    second = rms_norm(middle, channel_gain)
    gate_sum = jnp.dot(second, gather(gate_weight.astype(BF)), preferred_element_type=F32)
    up_sum = jnp.dot(second, gather(up_weight.astype(BF)), preferred_element_type=F32)
    hidden = (jax.nn.silu(gate_sum * gate_scale) * (up_sum * up_scale)).astype(BF)
    projected = transposed_product(hidden, gather(down_weight.astype(BF)))
    channel_part = (projected * down_feature).astype(BF)
    channel_out = lax.psum(channel_part, "tp").astype(F32)
    return (middle.astype(F32) + channel_out).astype(BF)


VMEM = pl.BlockSpec(memory_space=pltpu.VMEM)
SMEM = pl.BlockSpec(memory_space=pltpu.SMEM)
HBM = pl.BlockSpec(memory_space=pltpu.HBM)


def room(mebibytes):
    return pltpu.CompilerParams(vmem_limit_bytes=mebibytes << 20)


def packed_pair(gate, up, keep):
    aligned = keep // 128 * 128
    pieces = [gate[:, :aligned], up[:, :aligned]]
    if keep > aligned:
        gate_tail, up_tail = gate[:, aligned : aligned + 128], up[:, aligned : aligned + 128]
        lane = lax.broadcasted_iota(jnp.int32, gate_tail.shape, 1)
        pieces.append(jnp.where(lane < keep - aligned, gate_tail, pltpu.roll(up_tail, keep - aligned, 1)))
    return pieces


def pack_kernel(place, gate, up, gate_scale, up_scale, kept, sent, scale):
    keep = kept.shape[1] // 2

    def put(out, gates, ups):
        at = 0
        for piece in packed_pair(gates, ups, keep):
            out[:, at : at + piece.shape[1]] = piece.astype(out.dtype)
            at += piece.shape[1]

    low = (gate[...], up[...])
    high = tuple(pltpu.roll(v, keep, 1) for v in low)
    scales = tuple(jnp.broadcast_to(v[...], (8, 2 * keep)) for v in (gate_scale, up_scale))
    high_scales = tuple(pltpu.roll(v, keep, 1) for v in scales)

    @pl.when(place[1] == 0)
    def _():
        put(kept, *low)
        put(sent, *high)
        put(scale, *scales)

    @pl.when(place[1] != 0)
    def _():
        put(kept, *high)
        put(sent, *low)
        put(scale, *high_scales)


def run_pack(place, gate, up, gate_scale, up_scale):
    rows, width = gate.shape
    both = width // 2
    block = min(rows, 64)
    weight = pl.BlockSpec((block, both), lambda i, p: (i, p[0]))
    scale = pl.BlockSpec((1, both), lambda i, p: (0, p[0]))
    out = pl.BlockSpec((block, both), lambda i, p: (i, 0))
    shape = jax.ShapeDtypeStruct((rows, both), BF)
    return pl.pallas_call(
        pack_kernel,
        grid_spec=pltpu.PrefetchScalarGridSpec(
            num_scalar_prefetch=1,
            grid=(rows // block,),
            in_specs=[weight, weight, scale, scale],
            out_specs=(out, out, pl.BlockSpec((8, both), lambda i, p: (0, 0))),
        ),
        out_shape=(shape, shape, jax.ShapeDtypeStruct((8, both), F32)),
        compiler_params=room(12),
        name="pack",
        cost_estimate=pl.CostEstimate(flops=3_000_000_000, bytes_accessed=5_000_000, transcendentals=0),
    )(place, gate, up, gate_scale, up_scale)


def turn_kernel(place, down, kept, sent):
    keep = kept.shape[0]
    low, high = (down[:, i * keep : (i + 1) * keep].T.astype(BF) for i in range(2))

    @pl.when(place[1] == 0)
    def _():
        kept[...] = low
        sent[...] = high

    @pl.when(place[1] != 0)
    def _():
        kept[...] = high
        sent[...] = low


def run_turn(place, down):
    rows, width = down.shape
    block = 128
    out = pl.BlockSpec((width // 4, block), lambda i, p: (0, i))
    shape = jax.ShapeDtypeStruct((width // 4, rows), BF)
    return pl.pallas_call(
        turn_kernel,
        grid_spec=pltpu.PrefetchScalarGridSpec(
            num_scalar_prefetch=1,
            grid=(rows // block,),
            in_specs=[pl.BlockSpec((block, width // 2), lambda i, p: (i, p[0]))],
            out_specs=(out, out),
        ),
        out_shape=(shape, shape),
        compiler_params=room(12),
        name="turn",
        cost_estimate=pl.CostEstimate(flops=2_000_000_000, bytes_accessed=3_000_000, transcendentals=0),
    )(place, down)


def mixer_kernel(n_ring, half, *refs):
    place, normed, in_scale, mix, mix_scale = refs[:5]
    scales = refs[5 : 5 + n_ring]
    own, other = refs[5 + n_ring : 7 + n_ring]
    rest = refs[7 + n_ring : 7 + n_ring + 4 * (n_ring - 1)]
    part_mine, part_away, weights, packed, sems = refs[7 + n_ring + 4 * (n_ring - 1) :]
    rep, col, core = place[0], place[1], place[2]
    copies = []

    def bring(source, ring, y, h, rows):
        start = pl.multiple_of(ring * 4 * half + y * 2 * half + h * half, half)
        copy = pltpu.make_async_copy(
            source, weights.at[:, pl.ds(start, rows), :], sems.at[len(copies)]
        )
        copy.start()
        copies.append(copy)

    bring(own, 0, col, 0, 2 * half)
    bring(other, 0, 1 - col, 0, 2 * half)
    for k in range(1, n_ring):
        mine, across, beside, corner = rest[4 * (k - 1) : 4 * k]
        bring(mine, k, col, rep, half)
        bring(across, k, col, 1 - rep, half)
        bring(beside, k, 1 - col, rep, half)
        bring(corner, k, 1 - col, 1 - rep, half)
    for copy in copies:
        copy.wait()
    pool_in = jnp.dot(normed[...], weights[0], preferred_element_type=F32)
    pool_in = (pool_in * in_scale[...]).astype(BF)
    length, width = pool_in.shape
    offsets = lax.broadcasted_iota(jnp.int32, (length, length), 0) - lax.broadcasted_iota(
        jnp.int32, (length, length), 1
    )
    places = lax.broadcasted_iota(jnp.int32, (length, 1), 0)
    block = mix.shape[0]
    grouped = []
    for piece in range(width // POOL_GROUP):
        window = lax.shift_left(jnp.int32(2), core * (width // POOL_GROUP) + piece)
        band = jnp.where((offsets >= 0) & (offsets < window), 1.0, 0.0).astype(BF)
        columns = pool_in[:, piece * POOL_GROUP : (piece + 1) * POOL_GROUP]
        sums = jnp.dot(band, columns, preferred_element_type=F32)
        counts = jnp.minimum(places + 1, window).astype(F32)
        pooled = (sums / counts - columns.astype(F32)).astype(BF)
        for b in range(POOL_GROUP // block):
            lo = piece * POOL_GROUP + b * block
            mixed = jnp.dot(
                pooled[:, b * block : (b + 1) * block],
                mix[:, lo : lo + block].astype(BF),
                preferred_element_type=F32,
            )
            grouped.append((mixed * mix_scale[:, lo : lo + block]).astype(BF))
    packed[...] = jnp.concatenate(grouped, axis=1)
    rows = length // 2
    for out, h in ((part_away, 1 - core), (part_mine, core)):
        grouped = packed[pl.ds(pl.multiple_of(h * rows, rows), rows), :]
        for k in range(n_ring):
            for j in range(2):
                y = col if j == 0 else 1 - col
                at = pl.ds(pl.multiple_of((2 * k + y) * 2 * half, 2 * half), 2 * half)
                sums = transposed_product(grouped, weights[1, at, :])
                out[:, at] = (sums * scales[k][j, 0:1, :]).astype(BF)


def run_mixer(place, normed, in_scale, mix, mix_scale, scales, own, other, rest):
    length, width = normed.shape
    half = own.shape[1] // 2
    n_ring = len(scales)
    n_copies = 2 + len(rest)
    shape = jax.ShapeDtypeStruct((length // 2, width), BF)
    return pl.pallas_call(
        functools.partial(mixer_kernel, n_ring, half),
        out_shape=(shape, shape),
        in_specs=[SMEM] + [VMEM] * (4 + n_ring) + [HBM] * n_copies,
        out_specs=(VMEM, VMEM),
        scratch_shapes=[
            pltpu.VMEM((2, width, own.shape[2]), BF),
            pltpu.VMEM((length, own.shape[2]), BF),
            pltpu.SemaphoreType.DMA((n_copies,)),
        ],
        compiler_params=room(24),
        name="mixer",
        cost_estimate=pl.CostEstimate(flops=5_000_000_000, bytes_accessed=10_000_000, transcendentals=512),
    )(place, normed, in_scale, mix, mix_scale, *scales, own, other, *rest)


def normed_rows(floats, gain):
    scaled = floats * lax.rsqrt(jnp.mean(floats * floats, axis=-1, keepdims=True) + epsilon)
    return (scaled * gain).astype(BF)


def turn_into(n_ring, ring, source, out):
    block = out.shape[1] // n_ring
    for k in range(n_ring):
        at = lax.rem(ring - k + n_ring, n_ring) * block
        out[:, k * block : (k + 1) * block] = source[:, pl.ds(pl.multiple_of(at, block), block)]


def ready_kernel(n_ring, place, tokens, gain, next_gain, turned, normed, turned_gain, own_gain):
    turn_into(n_ring, place[3], tokens, turned)
    turn_into(n_ring, place[3], gain, own_gain)
    turn_into(n_ring, place[3], next_gain, turned_gain)
    normed[...] = normed_rows(turned[...].astype(F32), own_gain[...])


def run_ready(place, n_ring, tokens, gain, next_gain):
    length, width = tokens.shape
    block = length // 4
    rows = pl.BlockSpec((block, width), lambda i, p: (i, 0))
    line = pl.BlockSpec((1, width), lambda i, p: (0, 0))
    shape = jax.ShapeDtypeStruct((length, width), BF)
    return pl.pallas_call(
        functools.partial(ready_kernel, n_ring),
        grid_spec=pltpu.PrefetchScalarGridSpec(
            num_scalar_prefetch=1,
            grid=(4,),
            in_specs=[rows, line, line],
            out_specs=(rows, rows, line),
            scratch_shapes=[pltpu.VMEM((1, width), F32)],
        ),
        out_shape=(shape, shape, jax.ShapeDtypeStruct((1, width), F32)),
        compiler_params=room(16),
        name="ready",
        cost_estimate=pl.CostEstimate(flops=3_000_000_000, bytes_accessed=6_000_000, transcendentals=512),
    )(place, tokens, gain, next_gain)


def settle_kernel(place, tokens, part, other, gain, middle_mine, here):
    mixer_out = part[...].astype(F32) + other[...].astype(F32)
    middle = (tokens[...].astype(F32) + mixer_out).astype(BF)
    middle_mine[...] = middle
    here[...] = normed_rows(middle.astype(F32), gain[...])


def run_settle(place, tokens, part, other, gain):
    rows, width = part.shape
    block = rows // 4
    shape = jax.ShapeDtypeStruct((rows, width), BF)
    spec = pl.BlockSpec((block, width), lambda i, p: (i, 0))
    return pl.pallas_call(
        settle_kernel,
        grid_spec=pltpu.PrefetchScalarGridSpec(
            num_scalar_prefetch=1,
            grid=(4,),
            in_specs=[
                pl.BlockSpec((block, width), lambda i, p: (p[2] * 4 + i, 0)), spec, spec,
                pl.BlockSpec((1, width), lambda i, p: (0, 0)),
            ],
            out_specs=(spec, spec),
        ),
        out_shape=(shape, shape),
        compiler_params=room(16),
        name="settle",
        cost_estimate=pl.CostEstimate(flops=3_000_000_000, bytes_accessed=9_000_000, transcendentals=512),
    )(place, tokens, part, other, gain)


def gated_kernel(n_rows, starts, n_weights, *refs):
    place, scale, other_scale = refs[:3]
    rows = refs[3 : 3 + n_rows]
    parts = refs[3 + n_rows : 3 + n_rows + n_weights]
    hidden, weights, stage, row_sems, sems = refs[3 + n_rows + n_weights :]
    shard, both = parts[0].shape
    keep = both // 2
    aligned = keep // 128 * 128
    tail = keep - aligned
    copies = []
    for i, p in enumerate(parts):
        y = place[1] if i // 2 % 2 == 0 else 1 - place[1]
        at = pl.ds(pl.multiple_of((i // 4 * 2 + y) * shard, shard), shard)
        lanes = pl.ds(i % 2 * both, both)
        copies.append(pltpu.make_async_copy(p, weights.at[at, lanes], sems.at[i]))
    row_copies = [
        pltpu.make_async_copy(r, stage.at[pl.ds(start, r.shape[0]), :], row_sems.at[i])
        for i, (r, start) in enumerate(zip(rows, starts))
    ]
    for copy in row_copies:
        copy.start()
    for j in range(2):
        for copy in copies[j::2]:
            copy.start()
    for copy in row_copies:
        copy.wait()

    def product(lo, size):
        return jnp.dot(stage[...], weights[:, lo : lo + size], preferred_element_type=F32)

    for j in range(2):
        for copy in copies[j::2]:
            copy.wait()
        line = (scale, other_scale)[j]
        at = 0
        while at < aligned:
            size = min(256, aligned - at)
            gate = product(j * both + at, size) * line[0:1, at : at + size]
            up_at = aligned + at
            up = product(j * both + up_at, size) * line[0:1, up_at : up_at + size]
            hidden[:, j * aligned + at : j * aligned + at + size] = (jax.nn.silu(gate) * up).astype(BF)
            at += size
    if tail:
        first, second = (
            product(j * both + 2 * aligned, 2 * tail) * line[0:1, 2 * aligned :]
            for j, line in enumerate((scale, other_scale))
        )
        lane = lax.broadcasted_iota(jnp.int32, first.shape, 1)
        gate = jnp.where(lane < tail, first, pltpu.roll(second, tail, 1))
        up = jnp.where(lane < tail, pltpu.roll(first, tail, 1), second)
        hidden[:, 2 * aligned :] = (jax.nn.silu(gate) * up).astype(BF)


def run_gated(place, scale, other_scale, rows, parts):
    starts, total = [], 0
    for r in rows:
        starts.append(total)
        total += r.shape[0]
    width = rows[0].shape[1]
    both = parts[0].shape[1]
    return pl.pallas_call(
        functools.partial(gated_kernel, len(rows), tuple(starts), len(parts)),
        out_shape=jax.ShapeDtypeStruct((total, both), BF),
        in_specs=[SMEM, VMEM, VMEM] + [HBM] * (len(rows) + len(parts)),
        out_specs=VMEM,
        scratch_shapes=[
            pltpu.VMEM((width, 2 * both), BF),
            pltpu.VMEM((total, width), BF),
            pltpu.SemaphoreType.DMA((len(rows),)),
            pltpu.SemaphoreType.DMA((len(parts),)),
        ],
        compiler_params=room(34),
        name="gated",
        cost_estimate=pl.CostEstimate(flops=12_000_000_000, bytes_accessed=20_000_000, transcendentals=1_500_000),
    )(place, scale, other_scale, *rows, *parts)


def keep_kernel(k, place, hidden, scale, middle, *refs):
    parts = refs[:4]
    base, outs = refs[4], refs[5:8]
    ends = refs[8]
    keep, width = parts[0].shape
    aligned = keep // 128 * 128
    tail = keep - aligned
    rows = base.shape[0]
    for i in range(2):
        own, other = parts[2 * i : 2 * i + 2]
        y = place[1] if i == 0 else 1 - place[1]
        lanes = pl.ds(pl.multiple_of(y * width, width), width)
        from_lanes = pl.ds(pl.multiple_of((2 * k + y) * width, width), width)
        ends[:tail, :] = own[aligned:, :]
        ends[tail:, :] = other[aligned:, :]
        total = jnp.dot(hidden[:, :aligned], own[:aligned, :], preferred_element_type=F32)
        total += jnp.dot(
            hidden[:, aligned : 2 * aligned], other[:aligned, :], preferred_element_type=F32
        )
        total += jnp.dot(hidden[:, 2 * aligned :], ends[...], preferred_element_type=F32)
        total = total * scale[i, 1:2, :]
        base[:, lanes] = total[:rows, :] + middle[:, from_lanes].astype(F32)
        for j, out in enumerate(outs):
            out[:, lanes] = total[(j + 1) * rows : (j + 2) * rows, :].astype(BF)


def run_keep(place, hidden, scale, middle, parts, k):
    rows = hidden.shape[0] // 4
    keep, width = parts[0].shape
    shape = jax.ShapeDtypeStruct((rows, 2 * width), BF)
    return pl.pallas_call(
        functools.partial(keep_kernel, k),
        in_specs=[SMEM] + [VMEM] * 7,
        out_specs=(VMEM, VMEM, VMEM, VMEM),
        scratch_shapes=[pltpu.VMEM((2 * (keep % 128), width), BF)],
        out_shape=(jax.ShapeDtypeStruct(shape.shape, F32), shape, shape, shape),
        compiler_params=room(20),
        name="keep",
        cost_estimate=pl.CostEstimate(flops=2_000_000_000, bytes_accessed=5_000_000, transcendentals=0),
    )(place, hidden, scale, middle, *parts)


def join_kernel(base, first, second, third, out):
    total = base[...] + first[...].astype(F32) + second[...].astype(F32) + third[...].astype(F32)
    out[...] = total.astype(BF)


def run_join(base, *others):
    return pl.pallas_call(
        join_kernel,
        in_specs=[VMEM] * 4,
        out_specs=VMEM,
        out_shape=jax.ShapeDtypeStruct(base.shape, BF),
        compiler_params=room(8),
        name="join",
        cost_estimate=pl.CostEstimate(flops=1_000_000_000, bytes_accessed=2_000_000, transcendentals=0),
    )(base, *others)


def collect_kernel(n_ring, steps, *refs):
    place = refs[0]
    pieces = refs[1 : 1 + 2 * len(steps)]
    out, sems = refs[-2:]
    rows, width = pieces[0].shape
    copies = []
    for i, piece in enumerate(pieces):
        h = place[2] if i % 2 == 0 else 1 - place[2]
        block = lax.rem(place[3] - steps[i // 2] + n_ring, n_ring)
        at = out.at[
            pl.ds(pl.multiple_of(h * rows, rows), rows),
            pl.ds(pl.multiple_of(block * width, width), width),
        ]
        copy = pltpu.make_async_copy(piece, at, sems.at[i])
        copy.start()
        copies.append(copy)
    for copy in copies:
        copy.wait()


def run_collect(place, n_ring, steps, pieces, into=None):
    rows, width = pieces[0].shape
    extra = [] if into is None else [into]
    return pl.pallas_call(
        functools.partial(collect_kernel, n_ring, steps),
        out_shape=jax.ShapeDtypeStruct((2 * rows, width * n_ring), BF),
        in_specs=[SMEM] + [VMEM] * len(pieces) + [HBM] * len(extra),
        out_specs=HBM,
        input_output_aliases={1 + len(pieces): 0} if extra else {},
        scratch_shapes=[pltpu.SemaphoreType.DMA((len(pieces),))],
        compiler_params=room(12),
        name="collect",
        cost_estimate=pl.CostEstimate(flops=2_000_000_000, bytes_accessed=4_000_000, transcendentals=0),
    )(place, *pieces, *extra)


def shared_body(
    n_fs,
    tokens, mixer_gain, pool_input, input_scale, group_mix, group_scale, pool_output, output_scale,
    channel_gain, gate_weight, gate_scale, up_weight, up_scale, down_weight, down_scale,
):
    n_ring = n_fs // 2
    rep, fs, core = lax.axis_index("rep"), lax.axis_index("fs"), lax.axis_index("tp")
    ring, col = fs // 2, fs % 2
    half = pool_input.shape[0] // 2
    rows = tokens.shape[0] // 2

    swap = [(0, 1), (1, 0)]
    col_swap = [(i, i ^ 1) for i in range(n_fs)]
    diagonal = [
        (a * n_fs + i, (1 - a) * n_fs + (i ^ 1)) for a in range(2) for i in range(n_fs)
    ]

    def across(value):
        return lax.ppermute(value, "rep", swap)

    def beside(value):
        return lax.ppermute(value, "fs", col_swap)

    def corner(value):
        return lax.ppermute(value, ("rep", "fs"), diagonal)

    def partner(value):
        return lax.ppermute(value, "tp", swap)

    def around(value, steps=1):
        return lax.ppermute(
            value, "fs", [(i, (i + 2 * steps) % n_fs) for i in range(n_fs)]
        )

    place = jnp.stack([rep, col, core, ring]).astype(jnp.int32)

    own = jnp.stack([pool_input.astype(BF), pool_output.astype(BF)])
    mine = [lax.dynamic_slice_in_dim(own, rep * half, half, axis=1)]
    mine += [around(mine[0])]
    mine += [around(mine[1], k - 1) for k in range(2, n_ring - 1)]
    mine += [around(mine[0], -1)]
    other = beside(own)
    rest = []
    for k in range(1, n_ring):
        next_to, facing = beside(mine[k]), across(mine[k])
        last = across(next_to)
        rest += [mine[k], facing, next_to, last]

    own_scale = jnp.stack([output_scale, down_scale])
    pair = jnp.stack([own_scale, beside(own_scale)])
    scales = [pair] + [around(pair, k) for k in range(1, n_ring)]

    def streams(kept, sent):
        chains = []
        for start in (kept, beside(sent)):
            chain = [start]
            for _ in range(1, n_ring):
                chain.append(around(chain[-1]))
            chains.append([(c, partner(c)) for c in chain])
        return [chains[0][k] + chains[1][k] for k in range(n_ring)]

    gated_kept, gated_sent, gated_scale = run_pack(place, gate_weight, up_weight, gate_scale[None], up_scale[None])
    gated_parts = streams(gated_kept, gated_sent)
    down_parts = streams(*run_turn(place, down_weight))

    tokens, normed, next_gain = run_ready(place, n_ring, tokens, mixer_gain[None], channel_gain[None])
    part_mine, part_away = run_mixer(
        place, normed, input_scale[None], group_mix, group_scale[None], scales, own,
        other, rest,
    )
    middle_mine, here = run_settle(place, tokens, part_mine, partner(part_away), next_gain)

    ax, ay = across(here), beside(here)
    cut = rows // 2
    far = [across(ay[:cut]), beside(ax[cut:])]
    hidden = run_gated(
        place, gated_scale, partner(gated_scale), [here, ax, ay] + far,
        sum(gated_parts, ()),
    )

    pieces = []
    for k in range(n_ring):
        base, to_x, to_y, to_far = run_keep(place, hidden, scales[k], middle_mine, down_parts[k], k)
        total = run_join(
            base, across(to_x), beside(to_y),
            corner(to_far),
        )
        pieces.append((total, partner(total)))
    early = run_collect(place, n_ring, tuple(range(n_ring - 1)), sum(pieces[:-1], ()))
    return run_collect(place, n_ring, (n_ring - 1,), pieces[-1], early)


def solution(mesh):
    in_specs = (
        P(("rep", "fs"), None), P(), P("fs", "tp"), P("tp"), P(None, "tp"), P("tp"), P("fs", "tp"),
        P("fs"), P(), P("fs", "tp"), P("tp"), P("fs", "tp"), P("tp"), P("fs", "tp"), P("fs"),
    )
    out_specs = P(("rep", "fs"), None)
    n_rep, n_fs, n_tp = (mesh.shape[a] for a in ("rep", "fs", "tp"))
    shared = n_rep == 2 and n_tp == 2 and n_fs == 8

    def body(*args):
        return shared_body(n_fs, *args) if shared else plain_body(*args)

    return jax.shard_map(body, mesh=mesh, in_specs=in_specs, out_specs=out_specs, check_vma=False)
```

profile of v0, /device:TPU:0, one launch (start us, length us, event | category | flops | bytes accessed | tf_op | source)
XLA Modules:
  0.0 280.5 jit_solution(10778184148454902169)
XLA Ops:
  1.4 3.1 %collective-permute-start.6 = (bf16[2,128,512]{2,1,0:T(8,128)(2,1)S(1)}, bf16[2,128,512]{2,1,0:T(8,128)(2,1)S(1)}, u32[]{:S(2)}, u32[]{:S(2)}) collective-permute-start(bf16[2,128,512]{2,1,0:T(8,128)(2,1)S(1)} %fusion), channel_id=1, source_target_pairs={{0,4},{2,6},{4,8},{6,10},{8,12},{10,14},{12,0},{14,2},{1,5},{3,7},... | collective-permute-start | bytes 786440 | tf_op jit(solution)/shard_map/ppermute | solution.py:538
  4.5 2.1 collective-permute-start.14
  8.5 5.2 %collective-permute-done.6.refs_11_ = bf16[2,128,512]{2,1,0:T(8,128)(2,1)S(1)} collective-permute-done((bf16[2,128,512]{2,1,0:T(8,128)(2,1)S(1)}, bf16[2,128,512]{2,1,0:T(8,128)(2,1)S(1)}, u32[]{:S(2)}, u32[]{:S(2)}) %collective-permute-start.6) | collective-permute-done | bytes 262176 | tf_op jit(solution)/shard_map/ppermute | solution.py:538
  20.9 4.8 %collective-permute-start.2 = (f32[2,2,256]{2,1,0:T(2,128)S(1)}, f32[2,2,256]{2,1,0:T(2,128)S(1)}, u32[]{:S(2)}, u32[]{:S(2)}) collective-permute-start(f32[2,2,256]{2,1,0:T(2,128)S(1)} %pad_maximum_fusion.1.refs_5_.scale), channel_id=1, source_target_pairs={{0,4},{2,6},{4,8},{6,10},{8,12},{10,14},{12,0},{14,2},{1,5},{3,7},... | collective-permute-start | bytes 12296 | tf_op jit(solution)/shard_map/ppermute | solution.py:538
  25.7 2.4 collective-permute-done.2.refs_6_.scale
  28.1 2.6 collective-permute-start.3
  32.6 2.0 collective-permute-start.4
  40.9 6.0 %collective-permute-done.16.refs_21_ = bf16[2,128,512]{2,1,0:T(8,128)(2,1)S(1)} collective-permute-done((bf16[2,128,512]{2,1,0:T(8,128)(2,1)S(1)}, bf16[2,128,512]{2,1,0:T(8,128)(2,1)S(1)}, u32[]{:S(2)}, u32[]{:S(2)}) %collective-permute-start.16) | collective-permute-done | bytes 262176 | tf_op jit(solution)/shard_map/ppermute | solution.py:529
  48.9 2.1 collective-permute-done.15.refs_20_
  54.7 6.3 %collective-permute-done.5.refs_10_ = bf16[2,256,512]{2,1,0:T(8,128)(2,1)S(1)} collective-permute-done((bf16[2,256,512]{2,1,0:T(8,128)(2,1)S(1)}, bf16[2,256,512]{2,1,0:T(8,128)(2,1)S(1)}, u32[]{:S(2)}, u32[]{:S(2)}) %collective-permute-start.5) | collective-permute-done | bytes 524320 | tf_op jit(solution)/shard_map/ppermute | solution.py:529
  64.4 2.6 collective-permute-done.17.refs_22_
  67.6 2.3 collective-permute-done.13.refs_18_
  71.0 4.6 %mixer.1 = (bf16[256,2048]{1,0:T(8,128)(2,1)S(1)}, bf16[256,2048]{1,0:T(8,128)(2,1)S(1)}) custom-call(s32[4]{0:T(128)S(1)} %pad_add_fusion.place.refs_0_, bf16[512,2048]{1,0:T(8,128)(2,1)S(1)} %get-tuple-element.35.refs_1_, f32[1,512]{1,0:T(1,128)S(1)} %bitcast.19, f32[128,512]{1,0:T(8,128)S(1)} %copy-done.4, f32[1,512]{1,0:T(1,128)S(1)} %bitcast.20, ...), custom_call_target="tpu_custom_call" | custom-call | flops 5000000000 | bytes 10000000 | tf_op jit(solution)/shard_map/mixer/pallas_call | solution.py:249
  75.5 7.5 %collective-permute-done.42.refs_2_ = bf16[704,256]{1,0:T(8,128)(2,1)S(1)} collective-permute-done((bf16[704,256]{1,0:T(8,128)(2,1)S(1)}, bf16[704,256]{1,0:T(8,128)(2,1)S(1)}, u32[]{:S(2)}, u32[]{:S(2)}) %collective-permute-start.42) | collective-permute-done | bytes 360480 | tf_op jit(solution)/shard_map/ppermute | solution.py:529
  85.9 2.1 collective-permute-start.39
  88.0 23.5 %collective-permute-done.43.refs_2_ = bf16[704,256]{1,0:T(8,128)(2,1)S(1)} collective-permute-done((bf16[704,256]{1,0:T(8,128)(2,1)S(1)}, bf16[704,256]{1,0:T(8,128)(2,1)S(1)}, u32[]{:S(2)}, u32[]{:S(2)}) %collective-permute-start.43) | collective-permute-done | bytes 360480 | tf_op jit(solution)/shard_map/ppermute | solution.py:538
  111.6 7.7 %collective-permute-done.39.refs_0_ = bf16[704,256]{1,0:T(8,128)(2,1)S(1)} collective-permute-done((bf16[704,256]{1,0:T(8,128)(2,1)S(1)}, bf16[704,256]{1,0:T(8,128)(2,1)S(1)}, u32[]{:S(2)}, u32[]{:S(2)}) %collective-permute-start.39) | collective-permute-done | bytes 360480 | tf_op jit(solution)/shard_map/ppermute | solution.py:538
  120.3 14.4 %collective-permute-done.30.refs_16_ = bf16[256,1408]{1,0:T(8,128)(2,1)S(1)} collective-permute-done((bf16[256,1408]{1,0:T(8,128)(2,1)S(1)}, bf16[256,1408]{1,0:T(8,128)(2,1)S(1)}, u32[]{:S(2)}, u32[]{:S(2)}) %collective-permute-start.30) | collective-permute-done | bytes 720928 | tf_op jit(solution)/shard_map/ppermute | solution.py:538
  136.4 21.5 %collective-permute-done.44.refs_2_ = bf16[704,256]{1,0:T(8,128)(2,1)S(1)} collective-permute-done((bf16[704,256]{1,0:T(8,128)(2,1)S(1)}, bf16[704,256]{1,0:T(8,128)(2,1)S(1)}, u32[]{:S(2)}, u32[]{:S(2)}) %collective-permute-start.44) | collective-permute-done | bytes 360480 | tf_op jit(solution)/shard_map/ppermute | solution.py:538
  159.0 14.3 %collective-permute-done.34.refs_20_ = bf16[256,1408]{1,0:T(8,128)(2,1)S(1)} collective-permute-done((bf16[256,1408]{1,0:T(8,128)(2,1)S(1)}, bf16[256,1408]{1,0:T(8,128)(2,1)S(1)}, u32[]{:S(2)}, u32[]{:S(2)}) %collective-permute-start.34) | collective-permute-done | bytes 720928 | tf_op jit(solution)/shard_map/ppermute | solution.py:538
  173.4 15.2 %collective-permute-done.36.refs_22_ = bf16[256,1408]{1,0:T(8,128)(2,1)S(1)} collective-permute-done((bf16[256,1408]{1,0:T(8,128)(2,1)S(1)}, bf16[256,1408]{1,0:T(8,128)(2,1)S(1)}, u32[]{:S(2)}, u32[]{:S(2)}) %collective-permute-start.36) | collective-permute-done | bytes 720928 | tf_op jit(solution)/shard_map/ppermute | solution.py:538
  192.8 10.8 %collective-permute-done.21.refs_6_ = bf16[128,2048]{1,0:T(8,128)(2,1)S(1)} collective-permute-done((bf16[128,2048]{1,0:T(8,128)(2,1)S(1)}, bf16[128,2048]{1,0:T(8,128)(2,1)S(1)}, u32[]{:S(2)}, u32[]{:S(2)}) %collective-permute-start.21) | collective-permute-done | bytes 524320 | tf_op jit(solution)/shard_map/ppermute | solution.py:526
  203.9 17.7 %gated.1.hidden = bf16[1024,1408]{1,0:T(8,128)(2,1)S(1)} custom-call(s32[4]{0:T(128)S(1)} %pad_add_fusion.place.refs_0_, f32[8,1408]{1,0:T(8,128)S(1)} %get-tuple-element.33.refs_1_, f32[8,1408]{1,0:T(8,128)S(1)} %collective-permute-done.refs_2_, bf16[256,2048]{1,0:T(8,128)(2,1)S(1)} %get-tuple-element.39.refs_3_, ...), custom_call_target="tpu_custom_call" | custom-call | flops 12000000000 | bytes 20000000 | tf_op jit(solution)/shard_map/gated/pallas_call | solution.py:396
  222.7 2.6 keep.7
  226.9 2.6 keep.6
  233.6 2.7 keep.5
  237.8 6.6 %collective-permute-done.66.second = bf16[256,512]{1,0:T(8,128)(2,1)S(1)} collective-permute-done((bf16[256,512]{1,0:T(8,128)(2,1)S(1)}, bf16[256,512]{1,0:T(8,128)(2,1)S(1)}, u32[]{:S(2)}, u32[]{:S(2)}) %collective-permute-start.66) | collective-permute-done | bytes 262176 | tf_op jit(solution)/shard_map/ppermute | solution.py:529
  247.9 2.6 keep.4
  250.6 5.1 %collective-permute-done.60.second = bf16[256,512]{1,0:T(8,128)(2,1)S(1)} collective-permute-done((bf16[256,512]{1,0:T(8,128)(2,1)S(1)}, bf16[256,512]{1,0:T(8,128)(2,1)S(1)}, u32[]{:S(2)}, u32[]{:S(2)}) %collective-permute-start.60) | collective-permute-done | bytes 262176 | tf_op jit(solution)/shard_map/ppermute | solution.py:529
  257.2 2.1 collective-permute-start.49
  259.5 7.4 %collective-permute-done.54.second = bf16[256,512]{1,0:T(8,128)(2,1)S(1)} collective-permute-done((bf16[256,512]{1,0:T(8,128)(2,1)S(1)}, bf16[256,512]{1,0:T(8,128)(2,1)S(1)}, u32[]{:S(2)}, u32[]{:S(2)}) %collective-permute-start.54) | collective-permute-done | bytes 262176 | tf_op jit(solution)/shard_map/ppermute | solution.py:529
  268.5 8.5 %collective-permute-done.48.second = bf16[256,512]{1,0:T(8,128)(2,1)S(1)} collective-permute-done((bf16[256,512]{1,0:T(8,128)(2,1)S(1)}, bf16[256,512]{1,0:T(8,128)(2,1)S(1)}, u32[]{:S(2)}, u32[]{:S(2)}) %collective-permute-start.48) | collective-permute-done | bytes 262176 | tf_op jit(solution)/shard_map/ppermute | solution.py:529
  (158 shorter events, 58.9 us)
Async XLA Ops:
  4.5 33.2 %collective-permute-start.14 = (bf16[2,128,512]{2,1,0:T(8,128)(2,1)S(1)}, bf16[2,128,512]{2,1,0:T(8,128)(2,1)S(1)}, u32[]{:S(2)}, u32[]{:S(2)}) collective-permute-start(bf16[2,128,512]{2,1,0:T(8,128)(2,1)S(1)} %fusion), channel_id=1, source_target_pairs={{0,12},{2,14},{4,0},{6,2},{8,4},{10,6},{12,8},{14,10},{1,13},{3,15... | collective-permute-start | bytes 786440 | tf_op jit(solution)/shard_map/ppermute | solution.py:538
  13.7 25.1 %collective-permute-start.10 = (bf16[2,128,512]{2,1,0:T(8,128)(2,1)S(1)}, bf16[2,128,512]{2,1,0:T(8,128)(2,1)S(1)}, u32[]{:S(2)}, u32[]{:S(2)}) collective-permute-start(bf16[2,128,512]{2,1,0:T(8,128)(2,1)S(1)} %collective-permute-done.6.refs_11_), channel_id=1, source_target_pairs={{0,4},{2,6},{4,8},{6,10},{8,12},{10,14},{12,0},{14,2},{1,5},{3,7},... | collective-permute-start | bytes 786440 | tf_op jit(solution)/shard_map/ppermute | solution.py:538
  13.7 26.6 %collective-permute-start.8 = (bf16[2,128,512]{2,1,0:T(8,128)(2,1)S(1)}, bf16[2,128,512]{2,1,0:T(8,128)(2,1)S(1)}, u32[]{:S(2)}, u32[]{:S(2)}) collective-permute-start(bf16[2,128,512]{2,1,0:T(8,128)(2,1)S(1)} %collective-permute-done.6.refs_11_), channel_id=1, source_target_pairs={{0,2},{2,0},{4,6},{6,4},{8,10},{10,8},{12,14},{14,12},{1,3},{3,1},... | collective-permute-start | bytes 786440 | tf_op jit(solution)/shard_map/ppermute | solution.py:529
  40.3 20.7 %collective-permute-start.5 = (bf16[2,256,512]{2,1,0:T(8,128)(2,1)S(1)}, bf16[2,256,512]{2,1,0:T(8,128)(2,1)S(1)}, u32[]{:S(2)}, u32[]{:S(2)}) collective-permute-start(bf16[2,256,512]{2,1,0:T(8,128)(2,1)S(1)} %pad_maximum_fusion.refs_9_), channel_id=1, source_target_pairs={{0,2},{2,0},{4,6},{6,4},{8,10},{10,8},{12,14},{14,12},{1,3},{3,1},... | collective-permute-start | bytes 1572872 | tf_op jit(solution)/shard_map/ppermute | solution.py:529
  61.0 22.0 %collective-permute-start.24 = (bf16[256,1408]{1,0:T(8,128)(2,1)S(1)}, bf16[256,1408]{1,0:T(8,128)(2,1)S(1)}, u32[]{:S(2)}, u32[]{:S(2)}) collective-permute-start(bf16[256,1408]{1,0:T(8,128)(2,1)S(1)} %get-tuple-element.41), channel_id=1, source_target_pairs={{0,2},{2,0},{4,6},{6,4},{8,10},{10,8},{12,14},{14,12},{1,3},{3,1},... | collective-permute-start | bytes 2162696 | tf_op jit(solution)/shard_map/ppermute | solution.py:529
  61.6 24.3 %collective-permute-start.26 = (bf16[256,1408]{1,0:T(8,128)(2,1)S(1)}, bf16[256,1408]{1,0:T(8,128)(2,1)S(1)}, u32[]{:S(2)}, u32[]{:S(2)}) collective-permute-start(bf16[256,1408]{1,0:T(8,128)(2,1)S(1)} %get-tuple-element.40.refs_8_), channel_id=1, source_target_pairs={{0,4},{2,6},{4,8},{6,10},{8,12},{10,14},{12,0},{14,2},{1,5},{3,7},... | collective-permute-start | bytes 2162696 | tf_op jit(solution)/shard_map/ppermute | solution.py:538
  64.3 23.6 %collective-permute-start.23 = (bf16[256,1408]{1,0:T(8,128)(2,1)S(1)}, bf16[256,1408]{1,0:T(8,128)(2,1)S(1)}, u32[]{:S(2)}, u32[]{:S(2)}) collective-permute-start(bf16[256,1408]{1,0:T(8,128)(2,1)S(1)} %get-tuple-element.40.refs_8_), channel_id=1, source_target_pairs={{0,1},{1,0},{2,3},{3,2},{4,5},{5,4},{6,7},{7,6},{8,9},{9,8},{10,11... | collective-permute-start | bytes 2162696 | tf_op jit(solution)/shard_map/ppermute | solution.py:535
  83.0 51.7 %collective-permute-start.18 = (bf16[256,2048]{1,0:T(8,128)(2,1)S(1)}, bf16[256,2048]{1,0:T(8,128)(2,1)S(1)}, u32[]{:S(2)}, u32[]{:S(2)}) collective-permute-start(bf16[256,2048]{1,0:T(8,128)(2,1)S(1)} %get-tuple-element.37), channel_id=1, source_target_pairs={{0,1},{1,0},{2,3},{3,2},{4,5},{5,4},{6,7},{7,6},{8,9},{9,8},{10,11... | collective-permute-start | bytes 3145736 | tf_op jit(solution)/shard_map/ppermute | solution.py:535
  83.0 36.3 %collective-permute-start.28 = (bf16[256,1408]{1,0:T(8,128)(2,1)S(1)}, bf16[256,1408]{1,0:T(8,128)(2,1)S(1)}, u32[]{:S(2)}, u32[]{:S(2)}) collective-permute-start(bf16[256,1408]{1,0:T(8,128)(2,1)S(1)} %collective-permute-done.24.refs_10_), channel_id=1, source_target_pairs={{0,4},{2,6},{4,8},{6,10},{8,12},{10,14},{12,0},{14,2},{1,5},{3,7},... | collective-permute-start | bytes 2162696 | tf_op jit(solution)/shard_map/ppermute | solution.py:538
  84.1 27.4 %collective-permute-start.43 = (bf16[704,256]{1,0:T(8,128)(2,1)S(1)}, bf16[704,256]{1,0:T(8,128)(2,1)S(1)}, u32[]{:S(2)}, u32[]{:S(2)}) collective-permute-start(bf16[704,256]{1,0:T(8,128)(2,1)S(1)} %collective-permute-done.42.refs_2_), channel_id=1, source_target_pairs={{0,4},{2,6},{4,8},{6,10},{8,12},{10,14},{12,0},{14,2},{1,5},{3,7},... | collective-permute-start | bytes 1081352 | tf_op jit(solution)/shard_map/ppermute | solution.py:538
  85.9 33.4 %collective-permute-start.39 = (bf16[704,256]{1,0:T(8,128)(2,1)S(1)}, bf16[704,256]{1,0:T(8,128)(2,1)S(1)}, u32[]{:S(2)}, u32[]{:S(2)}) collective-permute-start(bf16[704,256]{1,0:T(8,128)(2,1)S(1)} %collective-permute-done.38.refs_0_), channel_id=1, source_target_pairs={{0,4},{2,6},{4,8},{6,10},{8,12},{10,14},{12,0},{14,2},{1,5},{3,7},... | collective-permute-start | bytes 1081352 | tf_op jit(solution)/shard_map/ppermute | solution.py:538
  87.9 46.8 %collective-permute-start.30 = (bf16[256,1408]{1,0:T(8,128)(2,1)S(1)}, bf16[256,1408]{1,0:T(8,128)(2,1)S(1)}, u32[]{:S(2)}, u32[]{:S(2)}) collective-permute-start(bf16[256,1408]{1,0:T(8,128)(2,1)S(1)} %collective-permute-done.26.refs_12_), channel_id=1, source_target_pairs={{0,4},{2,6},{4,8},{6,10},{8,12},{10,14},{12,0},{14,2},{1,5},{3,7},... | collective-permute-start | bytes 2162696 | tf_op jit(solution)/shard_map/ppermute | solution.py:538
  119.3 39.1 %collective-permute-start.25 = (bf16[256,1408]{1,0:T(8,128)(2,1)S(1)}, bf16[256,1408]{1,0:T(8,128)(2,1)S(1)}, u32[]{:S(2)}, u32[]{:S(2)}) collective-permute-start(bf16[256,1408]{1,0:T(8,128)(2,1)S(1)} %collective-permute-done.24.refs_10_), channel_id=1, source_target_pairs={{0,1},{1,0},{2,3},{3,2},{4,5},{5,4},{6,7},{7,6},{8,9},{9,8},{10,11... | collective-permute-start | bytes 2162696 | tf_op jit(solution)/shard_map/ppermute | solution.py:535
  119.3 39.7 %collective-permute-start.32 = (bf16[256,1408]{1,0:T(8,128)(2,1)S(1)}, bf16[256,1408]{1,0:T(8,128)(2,1)S(1)}, u32[]{:S(2)}, u32[]{:S(2)}) collective-permute-start(bf16[256,1408]{1,0:T(8,128)(2,1)S(1)} %collective-permute-done.28.refs_14_), channel_id=1, source_target_pairs={{0,4},{2,6},{4,8},{6,10},{8,12},{10,14},{12,0},{14,2},{1,5},{3,7},... | collective-permute-start | bytes 2162696 | tf_op jit(solution)/shard_map/ppermute | solution.py:538
  119.3 38.6 %collective-permute-start.44 = (bf16[704,256]{1,0:T(8,128)(2,1)S(1)}, bf16[704,256]{1,0:T(8,128)(2,1)S(1)}, u32[]{:S(2)}, u32[]{:S(2)}) collective-permute-start(bf16[704,256]{1,0:T(8,128)(2,1)S(1)} %collective-permute-done.43.refs_2_), channel_id=1, source_target_pairs={{0,4},{2,6},{4,8},{6,10},{8,12},{10,14},{12,0},{14,2},{1,5},{3,7},... | collective-permute-start | bytes 1081352 | tf_op jit(solution)/shard_map/ppermute | solution.py:538
  134.7 24.2 %collective-permute-start.27 = (bf16[256,1408]{1,0:T(8,128)(2,1)S(1)}, bf16[256,1408]{1,0:T(8,128)(2,1)S(1)}, u32[]{:S(2)}, u32[]{:S(2)}) collective-permute-start(bf16[256,1408]{1,0:T(8,128)(2,1)S(1)} %collective-permute-done.26.refs_12_), channel_id=1, source_target_pairs={{0,1},{1,0},{2,3},{3,2},{4,5},{5,4},{6,7},{7,6},{8,9},{9,8},{10,11... | collective-permute-start | bytes 2162696 | tf_op jit(solution)/shard_map/ppermute | solution.py:535
  134.7 38.6 %collective-permute-start.34 = (bf16[256,1408]{1,0:T(8,128)(2,1)S(1)}, bf16[256,1408]{1,0:T(8,128)(2,1)S(1)}, u32[]{:S(2)}, u32[]{:S(2)}) collective-permute-start(bf16[256,1408]{1,0:T(8,128)(2,1)S(1)} %collective-permute-done.30.refs_16_), channel_id=1, source_target_pairs={{0,4},{2,6},{4,8},{6,10},{8,12},{10,14},{12,0},{14,2},{1,5},{3,7},... | collective-permute-start | bytes 2162696 | tf_op jit(solution)/shard_map/ppermute | solution.py:538
  157.9 30.7 %collective-permute-start.20 = (bf16[256,2048]{1,0:T(8,128)(2,1)S(1)}, bf16[256,2048]{1,0:T(8,128)(2,1)S(1)}, u32[]{:S(2)}, u32[]{:S(2)}) collective-permute-start(bf16[256,2048]{1,0:T(8,128)(2,1)S(1)} %get-tuple-element.39.refs_3_), channel_id=1, source_target_pairs={{0,2},{2,0},{4,6},{6,4},{8,10},{10,8},{12,14},{14,12},{1,3},{3,1},... | collective-permute-start | bytes 3145736 | tf_op jit(solution)/shard_map/ppermute | solution.py:529
  158.4 30.7 %collective-permute-start.19 = (bf16[256,2048]{1,0:T(8,128)(2,1)S(1)}, bf16[256,2048]{1,0:T(8,128)(2,1)S(1)}, u32[]{:S(2)}, u32[]{:S(2)}) collective-permute-start(bf16[256,2048]{1,0:T(8,128)(2,1)S(1)} %get-tuple-element.39.refs_3_), channel_id=1, source_target_pairs={{0,16},{16,0},{1,17},{17,1},{2,18},{18,2},{3,19},{19,3},{4,20},{20... | collective-permute-start | bytes 3145736 | tf_op jit(solution)/shard_map/ppermute | solution.py:526
  159.0 29.6 %collective-permute-start.36 = (bf16[256,1408]{1,0:T(8,128)(2,1)S(1)}, bf16[256,1408]{1,0:T(8,128)(2,1)S(1)}, u32[]{:S(2)}, u32[]{:S(2)}) collective-permute-start(bf16[256,1408]{1,0:T(8,128)(2,1)S(1)} %collective-permute-done.32.refs_18_), channel_id=1, source_target_pairs={{0,4},{2,6},{4,8},{6,10},{8,12},{10,14},{12,0},{14,2},{1,5},{3,7},... | collective-permute-start | bytes 2162696 | tf_op jit(solution)/shard_map/ppermute | solution.py:538
  159.0 30.3 %collective-permute-start.29 = (bf16[256,1408]{1,0:T(8,128)(2,1)S(1)}, bf16[256,1408]{1,0:T(8,128)(2,1)S(1)}, u32[]{:S(2)}, u32[]{:S(2)}) collective-permute-start(bf16[256,1408]{1,0:T(8,128)(2,1)S(1)} %collective-permute-done.28.refs_14_), channel_id=1, source_target_pairs={{0,1},{1,0},{2,3},{3,2},{4,5},{5,4},{6,7},{7,6},{8,9},{9,8},{10,11... | collective-permute-start | bytes 2162696 | tf_op jit(solution)/shard_map/ppermute | solution.py:535
  190.8 34.5 %collective-permute-start.58 = (bf16[704,256]{1,0:T(8,128)(2,1)S(1)}, bf16[704,256]{1,0:T(8,128)(2,1)S(1)}, u32[]{:S(2)}, u32[]{:S(2)}) collective-permute-start(bf16[704,256]{1,0:T(8,128)(2,1)S(1)} %collective-permute-done.43.refs_2_), channel_id=1, source_target_pairs={{0,1},{1,0},{2,3},{3,2},{4,5},{5,4},{6,7},{7,6},{8,9},{9,8},{10,11... | collective-permute-start | bytes 1081352 | tf_op jit(solution)/shard_map/ppermute | solution.py:535
  191.8 29.8 %collective-permute-start.63 = (bf16[704,256]{1,0:T(8,128)(2,1)S(1)}, bf16[704,256]{1,0:T(8,128)(2,1)S(1)}, u32[]{:S(2)}, u32[]{:S(2)}) collective-permute-start(bf16[704,256]{1,0:T(8,128)(2,1)S(1)} %collective-permute-done.39.refs_0_), channel_id=1, source_target_pairs={{0,1},{1,0},{2,3},{3,2},{4,5},{5,4},{6,7},{7,6},{8,9},{9,8},{10,11... | collective-permute-start | bytes 1081352 | tf_op jit(solution)/shard_map/ppermute | solution.py:535
  192.8 29.1 %collective-permute-start.40 = (bf16[704,256]{1,0:T(8,128)(2,1)S(1)}, bf16[704,256]{1,0:T(8,128)(2,1)S(1)}, u32[]{:S(2)}, u32[]{:S(2)}) collective-permute-start(bf16[704,256]{1,0:T(8,128)(2,1)S(1)} %collective-permute-done.39.refs_0_), channel_id=1, source_target_pairs={{0,4},{2,6},{4,8},{6,10},{8,12},{10,14},{12,0},{14,2},{1,5},{3,7},... | collective-permute-start | bytes 1081352 | tf_op jit(solution)/shard_map/ppermute | solution.py:538
  203.6 18.6 %collective-permute-start.64 = (bf16[704,256]{1,0:T(8,128)(2,1)S(1)}, bf16[704,256]{1,0:T(8,128)(2,1)S(1)}, u32[]{:S(2)}, u32[]{:S(2)}) collective-permute-start(bf16[704,256]{1,0:T(8,128)(2,1)S(1)} %collective-permute-done.44.refs_2_), channel_id=1, source_target_pairs={{0,1},{1,0},{2,3},{3,2},{4,5},{5,4},{6,7},{7,6},{8,9},{9,8},{10,11... | collective-permute-start | bytes 1081352 | tf_op jit(solution)/shard_map/ppermute | solution.py:535
  203.9 18.6 %collective-permute-start.45 = (bf16[704,256]{1,0:T(8,128)(2,1)S(1)}, bf16[704,256]{1,0:T(8,128)(2,1)S(1)}, u32[]{:S(2)}, u32[]{:S(2)}) collective-permute-start(bf16[704,256]{1,0:T(8,128)(2,1)S(1)} %collective-permute-done.44.refs_2_), channel_id=1, source_target_pairs={{0,4},{2,6},{4,8},{6,10},{8,12},{10,14},{12,0},{14,2},{1,5},{3,7},... | collective-permute-start | bytes 1081352 | tf_op jit(solution)/shard_map/ppermute | solution.py:538
  233.1 22.5 %collective-permute-start.60 = (bf16[256,512]{1,0:T(8,128)(2,1)S(1)}, bf16[256,512]{1,0:T(8,128)(2,1)S(1)}, u32[]{:S(2)}, u32[]{:S(2)}) collective-permute-start(bf16[256,512]{1,0:T(8,128)(2,1)S(1)} %get-tuple-element.55), channel_id=1, source_target_pairs={{0,2},{2,0},{4,6},{6,4},{8,10},{10,8},{12,14},{14,12},{1,3},{3,1},... | collective-permute-start | bytes 786440 | tf_op jit(solution)/shard_map/ppermute | solution.py:529
  236.3 20.0 %collective-permute-start.61 = (bf16[256,512]{1,0:T(8,128)(2,1)S(1)}, bf16[256,512]{1,0:T(8,128)(2,1)S(1)}, u32[]{:S(2)}, u32[]{:S(2)}) collective-permute-start(bf16[256,512]{1,0:T(8,128)(2,1)S(1)} %get-tuple-element.56), channel_id=1, source_target_pairs={{0,18},{2,16},{4,22},{6,20},{8,26},{10,24},{12,30},{14,28},{16,2},... | collective-permute-start | bytes 786440 | tf_op jit(solution)/shard_map/ppermute | solution.py:532
  244.9 21.9 %collective-permute-start.54 = (bf16[256,512]{1,0:T(8,128)(2,1)S(1)}, bf16[256,512]{1,0:T(8,128)(2,1)S(1)}, u32[]{:S(2)}, u32[]{:S(2)}) collective-permute-start(bf16[256,512]{1,0:T(8,128)(2,1)S(1)} %get-tuple-element.51), channel_id=1, source_target_pairs={{0,2},{2,0},{4,6},{6,4},{8,10},{10,8},{12,14},{14,12},{1,3},{3,1},... | collective-permute-start | bytes 786440 | tf_op jit(solution)/shard_map/ppermute | solution.py:529
  245.9 20.9 %collective-permute-start.55 = (bf16[256,512]{1,0:T(8,128)(2,1)S(1)}, bf16[256,512]{1,0:T(8,128)(2,1)S(1)}, u32[]{:S(2)}, u32[]{:S(2)}) collective-permute-start(bf16[256,512]{1,0:T(8,128)(2,1)S(1)} %get-tuple-element.52), channel_id=1, source_target_pairs={{0,18},{2,16},{4,22},{6,20},{8,26},{10,24},{12,30},{14,28},{16,2},... | collective-permute-start | bytes 786440 | tf_op jit(solution)/shard_map/ppermute | solution.py:532
  256.3 20.6 %collective-permute-start.48 = (bf16[256,512]{1,0:T(8,128)(2,1)S(1)}, bf16[256,512]{1,0:T(8,128)(2,1)S(1)}, u32[]{:S(2)}, u32[]{:S(2)}) collective-permute-start(bf16[256,512]{1,0:T(8,128)(2,1)S(1)} %get-tuple-element.47), channel_id=1, source_target_pairs={{0,2},{2,0},{4,6},{6,4},{8,10},{10,8},{12,14},{14,12},{1,3},{3,1},... | collective-permute-start | bytes 786440 | tf_op jit(solution)/shard_map/ppermute | solution.py:529
  257.2 19.7 %collective-permute-start.49 = (bf16[256,512]{1,0:T(8,128)(2,1)S(1)}, bf16[256,512]{1,0:T(8,128)(2,1)S(1)}, u32[]{:S(2)}, u32[]{:S(2)}) collective-permute-start(bf16[256,512]{1,0:T(8,128)(2,1)S(1)} %get-tuple-element.48), channel_id=1, source_target_pairs={{0,18},{2,16},{4,22},{6,20},{8,26},{10,24},{12,30},{14,28},{16,2},... | collective-permute-start | bytes 786440 | tf_op jit(solution)/shard_map/ppermute | solution.py:532
  (50 other events, 584.5 us)
where the time goes:
time: 281 us; the launch traced here: 280 us
  waiting for transfers between devices  177 us (63%)
  starting transfers between devices  54.5 us (19%)
  Pallas kernels  42.9 us (15%)
  local copies, waits for them, and re-layouts  3.77 us (1%)
    ppermute x18, waiting for transfers between devices, around(): lax.ppermute(value, 'fs', [(i, (i + 2 * steps) % n_fs) for i in range(n_f...  108 us
    ppermute x13, waiting for transfers between devices, beside(): return lax.ppermute(value, 'fs', col_swap)  47.5 us
    ppermute x18, starting transfers between devices, around(): lax.ppermute(value, 'fs', [(i, (i + 2 * steps) % n_fs) for i in range(n_f...  23 us
    ppermute x12, waiting for transfers between devices, across(): return lax.ppermute(value, 'rep', swap)  19.6 us
    pallas_call x1, Pallas kernels, run_gated(): pl.pallas_call(functools.partial(gated_kernel, len(rows), tuple(starts),...  17.7 us
    ppermute x12, starting transfers between devices, across(): return lax.ppermute(value, 'rep', swap)  11.3 us
    pallas_call x4, Pallas kernels, run_keep(): pl.pallas_call(functools.partial(keep_kernel, k), in_specs=[SMEM] + [VMEM...  10.5 us
    ppermute x13, starting transfers between devices, beside(): return lax.ppermute(value, 'fs', col_swap)  10.4 us
  transfers between devices with their start and end apart: 69, of which 28 were waited for; matrix products, arithmetic and copies ran while one was open for 0% of the time, Pallas kernels for 15%

commit v1 on v0

--- a/solution.py
+++ b/solution.py
@@ -84,7 +84,9 @@
 
 def packed_pair(gate, up, keep):
     aligned = keep // 128 * 128
-    pieces = [gate[:, :aligned], up[:, :aligned]]
+    pieces = []
+    for at in range(0, aligned, 128):
+        pieces += [gate[:, at : at + 128], up[:, at : at + 128]]
     if keep > aligned:
         gate_tail, up_tail = gate[:, aligned : aligned + 128], up[:, aligned : aligned + 128]
         lane = lax.broadcasted_iota(jnp.int32, gate_tail.shape, 1)
@@ -342,20 +344,25 @@
     keep = both // 2
     aligned = keep // 128 * 128
     tail = keep - aligned
-    copies = []
+    batches = ([], [], [])
     for i, p in enumerate(parts):
         y = place[1] if i // 2 % 2 == 0 else 1 - place[1]
         at = pl.ds(pl.multiple_of((i // 4 * 2 + y) * shard, shard), shard)
-        lanes = pl.ds(i % 2 * both, both)
-        copies.append(pltpu.make_async_copy(p, weights.at[at, lanes], sems.at[i]))
+        main, end = i % 2 * 2 * aligned, 4 * aligned + i % 2 * 2 * tail
+        for batch, start, to, size in ((i % 2, 0, main, 2 * aligned), (2, 2 * aligned, end, 2 * tail)):
+            if size:
+                batches[batch].append(
+                    pltpu.make_async_copy(
+                        p.at[:, pl.ds(start, size)], weights.at[at, pl.ds(to, size)],
+                        sems.at[2 * i + batch // 2],
+                    )
+                )
     row_copies = [
         pltpu.make_async_copy(r, stage.at[pl.ds(start, r.shape[0]), :], row_sems.at[i])
         for i, (r, start) in enumerate(zip(rows, starts))
     ]
-    for copy in row_copies:
-        copy.start()
-    for j in range(2):
-        for copy in copies[j::2]:
+    for batch in (row_copies, *batches):
+        for copy in batch:
             copy.start()
     for copy in row_copies:
         copy.wait()
@@ -363,26 +370,24 @@
     def product(lo, size):
         return jnp.dot(stage[...], weights[:, lo : lo + size], preferred_element_type=F32)
 
-    for j in range(2):
-        for copy in copies[j::2]:
+    for j, line in enumerate((scale, other_scale)):
+        for copy in batches[j]:
             copy.wait()
-        line = (scale, other_scale)[j]
-        at = 0
-        while at < aligned:
-            size = min(256, aligned - at)
-            gate = product(j * both + at, size) * line[0:1, at : at + size]
-            up_at = aligned + at
-            up = product(j * both + up_at, size) * line[0:1, up_at : up_at + size]
-            hidden[:, j * aligned + at : j * aligned + at + size] = (jax.nn.silu(gate) * up).astype(BF)
-            at += size
+        for at in range(0, aligned, 128):
+            sums = product(2 * (j * aligned + at), 256) * line[0:1, 2 * at : 2 * at + 256]
+            gate, up = sums[:, :128], sums[:, 128:]
+            hidden[:, j * aligned + at : j * aligned + at + 128] = (jax.nn.silu(gate) * up).astype(BF)
     if tail:
-        first, second = (
-            product(j * both + 2 * aligned, 2 * tail) * line[0:1, 2 * aligned :]
+        for copy in batches[2]:
+            copy.wait()
+        sums = product(4 * aligned, 4 * tail)
+        own, other = (
+            sums[:, 2 * j * tail : 2 * (j + 1) * tail] * line[0:1, 2 * aligned :]
             for j, line in enumerate((scale, other_scale))
         )
-        lane = lax.broadcasted_iota(jnp.int32, first.shape, 1)
-        gate = jnp.where(lane < tail, first, pltpu.roll(second, tail, 1))
-        up = jnp.where(lane < tail, pltpu.roll(first, tail, 1), second)
+        lane = lax.broadcasted_iota(jnp.int32, own.shape, 1)
+        gate = jnp.where(lane < tail, own, pltpu.roll(other, tail, 1))
+        up = jnp.where(lane < tail, pltpu.roll(own, tail, 1), other)
         hidden[:, 2 * aligned :] = (jax.nn.silu(gate) * up).astype(BF)
 
 
@@ -402,7 +407,7 @@
             pltpu.VMEM((width, 2 * both), BF),
             pltpu.VMEM((total, width), BF),
             pltpu.SemaphoreType.DMA((len(rows),)),
-            pltpu.SemaphoreType.DMA((len(parts),)),
+            pltpu.SemaphoreType.DMA((2 * len(parts),)),
         ],
         compiler_params=room(34),
         name="gated",
@@ -411,15 +416,14 @@
 
 
 def keep_kernel(k, place, hidden, scale, middle, *refs):
-    parts = refs[:4]
-    base, outs = refs[4], refs[5:8]
-    ends = refs[8]
-    keep, width = parts[0].shape
+    both, both_other, base = refs[:3]
+    outs, ends = refs[3:6], refs[6]
+    _, keep, width = both.shape
     aligned = keep // 128 * 128
     tail = keep - aligned
     rows = base.shape[0]
     for i in range(2):
-        own, other = parts[2 * i : 2 * i + 2]
+        own, other = both.at[i], both_other.at[i]
         y = place[1] if i == 0 else 1 - place[1]
         lanes = pl.ds(pl.multiple_of(y * width, width), width)
         from_lanes = pl.ds(pl.multiple_of((2 * k + y) * width, width), width)
@@ -438,11 +442,11 @@
 
 def run_keep(place, hidden, scale, middle, parts, k):
     rows = hidden.shape[0] // 4
-    keep, width = parts[0].shape
+    _, keep, width = parts[0].shape
     shape = jax.ShapeDtypeStruct((rows, 2 * width), BF)
     return pl.pallas_call(
         functools.partial(keep_kernel, k),
-        in_specs=[SMEM] + [VMEM] * 7,
+        in_specs=[SMEM] + [VMEM] * 5,
         out_specs=(VMEM, VMEM, VMEM, VMEM),
         scratch_shapes=[pltpu.VMEM((2 * (keep % 128), width), BF)],
         out_shape=(jax.ShapeDtypeStruct(shape.shape, F32), shape, shape, shape),
@@ -557,18 +561,19 @@
     pair = jnp.stack([own_scale, beside(own_scale)])
     scales = [pair] + [around(pair, k) for k in range(1, n_ring)]
 
-    def streams(kept, sent):
-        chains = []
-        for start in (kept, beside(sent)):
-            chain = [start]
-            for _ in range(1, n_ring):
-                chain.append(around(chain[-1]))
-            chains.append([(c, partner(c)) for c in chain])
-        return [chains[0][k] + chains[1][k] for k in range(n_ring)]
+    def circled(start, back):
+        chain = [start, around(start)]
+        for _ in range(2, n_ring - back):
+            chain.append(around(chain[-1]))
+        if back:
+            chain.append(around(start, -1))
+        return [(c, partner(c)) for c in chain]
 
     gated_kept, gated_sent, gated_scale = run_pack(place, gate_weight, up_weight, gate_scale[None], up_scale[None])
-    gated_parts = streams(gated_kept, gated_sent)
-    down_parts = streams(*run_turn(place, down_weight))
+    own_column, next_column = circled(gated_kept, 0), circled(beside(gated_sent), 0)
+    gated_parts = [a + b for a, b in zip(own_column, next_column)]
+    down_kept, down_sent = run_turn(place, down_weight)
+    down_parts = circled(jnp.stack([down_kept, beside(down_sent)]), 1)
 
     tokens, normed, next_gain = run_ready(place, n_ring, tokens, mixer_gain[None], channel_gain[None])
     part_mine, part_away = run_mixer(
@@ -586,15 +591,16 @@
     )
 
     pieces = []
-    for k in range(n_ring):
+    steps = (0, 1) + tuple(range(n_ring - 1, 1, -1))
+    for k in steps:
         base, to_x, to_y, to_far = run_keep(place, hidden, scales[k], middle_mine, down_parts[k], k)
         total = run_join(
             base, across(to_x), beside(to_y),
             corner(to_far),
         )
         pieces.append((total, partner(total)))
-    early = run_collect(place, n_ring, tuple(range(n_ring - 1)), sum(pieces[:-1], ()))
-    return run_collect(place, n_ring, (n_ring - 1,), pieces[-1], early)
+    early = run_collect(place, n_ring, steps[:-1], sum(pieces[:-1], ()))
+    return run_collect(place, n_ring, steps[-1:], pieces[-1], early)
 
 
 def solution(mesh):

time: 281 us -> 294 us (1.046)
  starting transfers between devices: 54.5 us -> 65.2 us
  waiting for transfers between devices: 177 us -> 180 us
    ppermute x13, starting transfers between devices: 10.4 us -> 21.4 us  [beside(): return lax.ppermute(value, 'fs', col_swap)]
    ppermute x13, waiting for transfers between devices: 47.5 us -> 39.4 us  [beside(): return lax.ppermute(value, 'fs', col_swap)]
    ppermute x12, waiting for transfers between devices: 19.6 us -> 25.6 us  [across(): return lax.ppermute(value, 'rep', swap)]
    ppermute x18 -> x15, waiting for transfers between devices: 108 us -> 112 us  [around(): lax.ppermute(value, 'fs', [(i, (i + 2 * steps) % n_fs) for i in range(n_f...]
    ppermute x18 -> x15, starting transfers between devices: 23 us -> 23.1 us  [around(): lax.ppermute(value, 'fs', [(i, (i + 2 * steps) % n_fs) for i in range(n_f...]
  transfers between devices with their start and end apart: 69 -> 62, of which waited for: 28 -> 29; matrix products, arithmetic and copies ran while one was open for 0% -> 0% of each run, Pallas kernels for 15% -> 14%
where the time goes in v1:
time: 294 us
  waiting for transfers between devices  180 us (61%)
  starting transfers between devices  65.2 us (22%)
  Pallas kernels  42.4 us (14%)
  local copies, waits for them, and re-layouts  3.78 us (1%)
    ppermute x15, waiting for transfers between devices, around(): lax.ppermute(value, 'fs', [(i, (i + 2 * steps) % n_fs) for i in range(n_f...  112 us
    ppermute x13, waiting for transfers between devices, beside(): return lax.ppermute(value, 'fs', col_swap)  39.4 us
    ppermute x12, waiting for transfers between devices, across(): return lax.ppermute(value, 'rep', swap)  25.6 us
    ppermute x15, starting transfers between devices, around(): lax.ppermute(value, 'fs', [(i, (i + 2 * steps) % n_fs) for i in range(n_f...  23.1 us
    ppermute x13, starting transfers between devices, beside(): return lax.ppermute(value, 'fs', col_swap)  21.4 us
    pallas_call x1, Pallas kernels, run_gated(): pl.pallas_call(functools.partial(gated_kernel, len(rows), tuple(starts),...  16.9 us
    ppermute x12, starting transfers between devices, across(): return lax.ppermute(value, 'rep', swap)  13.4 us
    pallas_call x4, Pallas kernels, run_keep(): pl.pallas_call(functools.partial(keep_kernel, k), in_specs=[SMEM] + [VMEM...  10.8 us
  transfers between devices with their start and end apart: 62, of which 29 were waited for; matrix products, arithmetic and copies ran while one was open for 0% of the time, Pallas kernels for 14%

profile of v1, /device:TPU:0, one launch (start us, length us, event | category | flops | bytes accessed | tf_op | source)
XLA Modules:
  0.0 293.7 jit_solution(3053927161457546889)
XLA Ops:
  1.4 3.1 %collective-permute-start.6 = (bf16[2,128,512]{2,1,0:T(8,128)(2,1)S(1)}, bf16[2,128,512]{2,1,0:T(8,128)(2,1)S(1)}, u32[]{:S(2)}, u32[]{:S(2)}) collective-permute-start(bf16[2,128,512]{2,1,0:T(8,128)(2,1)S(1)} %fusion), channel_id=1, source_target_pairs={{0,4},{2,6},{4,8},{6,10},{8,12},{10,14},{12,0},{14,2},{1,5},{3,7},... | collective-permute-start | bytes 786440 | tf_op jit(solution)/shard_map/ppermute | solution.py:542
  27.2 3.6 %collective-permute-done.38 = bf16[704,256]{1,0:T(8,128)(2,1)S(1)} collective-permute-done((bf16[704,256]{1,0:T(8,128)(2,1)S(1)}, bf16[704,256]{1,0:T(8,128)(2,1)S(1)}, u32[]{:S(2)}, u32[]{:S(2)}) %collective-permute-start.38) | collective-permute-done | bytes 360480 | tf_op jit(solution)/shard_map/ppermute | solution.py:533
  32.8 14.8 %collective-permute-done.8.refs_13_ = bf16[2,128,512]{2,1,0:T(8,128)(2,1)S(1)} collective-permute-done((bf16[2,128,512]{2,1,0:T(8,128)(2,1)S(1)}, bf16[2,128,512]{2,1,0:T(8,128)(2,1)S(1)}, u32[]{:S(2)}, u32[]{:S(2)}) %collective-permute-start.8) | collective-permute-done | bytes 262176 | tf_op jit(solution)/shard_map/ppermute | solution.py:533
  48.3 5.0 %collective-permute-done.16.refs_21_ = bf16[2,128,512]{2,1,0:T(8,128)(2,1)S(1)} collective-permute-done((bf16[2,128,512]{2,1,0:T(8,128)(2,1)S(1)}, bf16[2,128,512]{2,1,0:T(8,128)(2,1)S(1)}, u32[]{:S(2)}, u32[]{:S(2)}) %collective-permute-start.16) | collective-permute-done | bytes 262176 | tf_op jit(solution)/shard_map/ppermute | solution.py:533
  63.3 5.4 %collective-permute-done.9.refs_14_ = bf16[2,128,512]{2,1,0:T(8,128)(2,1)S(1)} collective-permute-done((bf16[2,128,512]{2,1,0:T(8,128)(2,1)S(1)}, bf16[2,128,512]{2,1,0:T(8,128)(2,1)S(1)}, u32[]{:S(2)}, u32[]{:S(2)}) %collective-permute-start.9) | collective-permute-done | bytes 262176 | tf_op jit(solution)/shard_map/ppermute | solution.py:530
  68.7 3.6 %collective-permute-done.17.refs_22_ = bf16[2,128,512]{2,1,0:T(8,128)(2,1)S(1)} collective-permute-done((bf16[2,128,512]{2,1,0:T(8,128)(2,1)S(1)}, bf16[2,128,512]{2,1,0:T(8,128)(2,1)S(1)}, u32[]{:S(2)}, u32[]{:S(2)}) %collective-permute-start.17) | collective-permute-done | bytes 262176 | tf_op jit(solution)/shard_map/ppermute | solution.py:530
  72.3 3.3 %collective-permute-start.56 = (bf16[2,704,256]{2,1,0:T(8,128)(2,1)S(1)}, bf16[2,704,256]{2,1,0:T(8,128)(2,1)S(1)}, u32[]{:S(2)}, u32[]{:S(2)}) collective-permute-start(bf16[2,704,256]{2,1,0:T(8,128)(2,1)S(1)} %pad_maximum_fusion.refs_0_), channel_id=1, source_target_pairs={{0,12},{2,14},{4,0},{6,2},{8,4},{10,6},{12,8},{14,10},{1,13},{3,15... | collective-permute-start | bytes 2162696 | tf_op jit(solution)/shard_map/ppermute | solution.py:542
  76.9 4.6 %mixer.1 = (bf16[256,2048]{1,0:T(8,128)(2,1)S(1)}, bf16[256,2048]{1,0:T(8,128)(2,1)S(1)}) custom-call(s32[4]{0:T(128)S(1)} %pad_add_fusion.place.refs_0_, bf16[512,2048]{1,0:T(8,128)(2,1)S(1)} %get-tuple-element.35.refs_1_, f32[1,512]{1,0:T(1,128)S(1)} %bitcast.22, f32[128,512]{1,0:T(8,128)S(1)} %copy-done.4, f32[1,512]{1,0:T(1,128)S(1)} %bitcast.23, ...), custom_call_target="tpu_custom_call" | custom-call | flops 5000000000 | bytes 10000000 | tf_op jit(solution)/shard_map/mixer/pallas_call | solution.py:251
  83.9 5.4 %collective-permute-start.28 = (bf16[256,1408]{1,0:T(8,128)(2,1)S(1)}, bf16[256,1408]{1,0:T(8,128)(2,1)S(1)}, u32[]{:S(2)}, u32[]{:S(2)}) collective-permute-start(bf16[256,1408]{1,0:T(8,128)(2,1)S(1)} %collective-permute-done.24.refs_10_), channel_id=1, source_target_pairs={{0,4},{2,6},{4,8},{6,10},{8,12},{10,14},{12,0},{14,2},{1,5},{3,7},... | collective-permute-start | bytes 2162696 | tf_op jit(solution)/shard_map/ppermute | solution.py:542
  89.4 3.0 %collective-permute-start.30 = (bf16[256,1408]{1,0:T(8,128)(2,1)S(1)}, bf16[256,1408]{1,0:T(8,128)(2,1)S(1)}, u32[]{:S(2)}, u32[]{:S(2)}) collective-permute-start(bf16[256,1408]{1,0:T(8,128)(2,1)S(1)} %collective-permute-done.26.refs_12_), channel_id=1, source_target_pairs={{0,4},{2,6},{4,8},{6,10},{8,12},{10,14},{12,0},{14,2},{1,5},{3,7},... | collective-permute-start | bytes 2162696 | tf_op jit(solution)/shard_map/ppermute | solution.py:542
  92.4 7.0 %collective-permute-done.56.refs_0_ = bf16[2,704,256]{2,1,0:T(8,128)(2,1)S(1)} collective-permute-done((bf16[2,704,256]{2,1,0:T(8,128)(2,1)S(1)}, bf16[2,704,256]{2,1,0:T(8,128)(2,1)S(1)}, u32[]{:S(2)}, u32[]{:S(2)}) %collective-permute-start.56) | collective-permute-done | bytes 720928 | tf_op jit(solution)/shard_map/ppermute | solution.py:542
  99.4 15.4 %collective-permute-done.39.refs_0_ = bf16[2,704,256]{2,1,0:T(8,128)(2,1)S(1)} collective-permute-done((bf16[2,704,256]{2,1,0:T(8,128)(2,1)S(1)}, bf16[2,704,256]{2,1,0:T(8,128)(2,1)S(1)}, u32[]{:S(2)}, u32[]{:S(2)}) %collective-permute-start.39) | collective-permute-done | bytes 720928 | tf_op jit(solution)/shard_map/ppermute | solution.py:542
  114.8 15.4 %collective-permute-done.28.refs_14_ = bf16[256,1408]{1,0:T(8,128)(2,1)S(1)} collective-permute-done((bf16[256,1408]{1,0:T(8,128)(2,1)S(1)}, bf16[256,1408]{1,0:T(8,128)(2,1)S(1)}, u32[]{:S(2)}, u32[]{:S(2)}) %collective-permute-start.28) | collective-permute-done | bytes 720928 | tf_op jit(solution)/shard_map/ppermute | solution.py:542
  130.3 15.4 %collective-permute-done.30.refs_16_ = bf16[256,1408]{1,0:T(8,128)(2,1)S(1)} collective-permute-done((bf16[256,1408]{1,0:T(8,128)(2,1)S(1)}, bf16[256,1408]{1,0:T(8,128)(2,1)S(1)}, u32[]{:S(2)}, u32[]{:S(2)}) %collective-permute-start.30) | collective-permute-done | bytes 720928 | tf_op jit(solution)/shard_map/ppermute | solution.py:542
  148.4 12.8 %collective-permute-done.32.refs_18_ = bf16[256,1408]{1,0:T(8,128)(2,1)S(1)} collective-permute-done((bf16[256,1408]{1,0:T(8,128)(2,1)S(1)}, bf16[256,1408]{1,0:T(8,128)(2,1)S(1)}, u32[]{:S(2)}, u32[]{:S(2)}) %collective-permute-start.32) | collective-permute-done | bytes 720928 | tf_op jit(solution)/shard_map/ppermute | solution.py:542
  161.2 15.4 %collective-permute-done.40.refs_0_ = bf16[2,704,256]{2,1,0:T(8,128)(2,1)S(1)} collective-permute-done((bf16[2,704,256]{2,1,0:T(8,128)(2,1)S(1)}, bf16[2,704,256]{2,1,0:T(8,128)(2,1)S(1)}, u32[]{:S(2)}, u32[]{:S(2)}) %collective-permute-start.40) | collective-permute-done | bytes 720928 | tf_op jit(solution)/shard_map/ppermute | solution.py:542
  176.6 15.4 %collective-permute-done.34.refs_20_ = bf16[256,1408]{1,0:T(8,128)(2,1)S(1)} collective-permute-done((bf16[256,1408]{1,0:T(8,128)(2,1)S(1)}, bf16[256,1408]{1,0:T(8,128)(2,1)S(1)}, u32[]{:S(2)}, u32[]{:S(2)}) %collective-permute-start.34) | collective-permute-done | bytes 720928 | tf_op jit(solution)/shard_map/ppermute | solution.py:542
  192.1 10.1 %collective-permute-done.36.refs_22_ = bf16[256,1408]{1,0:T(8,128)(2,1)S(1)} collective-permute-done((bf16[256,1408]{1,0:T(8,128)(2,1)S(1)}, bf16[256,1408]{1,0:T(8,128)(2,1)S(1)}, u32[]{:S(2)}, u32[]{:S(2)}) %collective-permute-start.36) | collective-permute-done | bytes 720928 | tf_op jit(solution)/shard_map/ppermute | solution.py:542
  203.4 5.5 %collective-permute-start.22 = (bf16[128,2048]{1,0:T(8,128)(2,1)S(1)}, bf16[128,2048]{1,0:T(8,128)(2,1)S(1)}, u32[]{:S(2)}, u32[]{:S(2)}) collective-permute-start(bf16[128,2048]{1,0:T(8,128)(2,1)S(1)} %slice.9), channel_id=1, source_target_pairs={{0,2},{2,0},{4,6},{6,4},{8,10},{10,8},{12,14},{14,12},{1,3},{3,1},... | collective-permute-start | bytes 1572872 | tf_op jit(solution)/shard_map/ppermute | solution.py:533
  209.6 7.6 %collective-permute-done.21.refs_6_ = bf16[128,2048]{1,0:T(8,128)(2,1)S(1)} collective-permute-done((bf16[128,2048]{1,0:T(8,128)(2,1)S(1)}, bf16[128,2048]{1,0:T(8,128)(2,1)S(1)}, u32[]{:S(2)}, u32[]{:S(2)}) %collective-permute-start.21) | collective-permute-done | bytes 524320 | tf_op jit(solution)/shard_map/ppermute | solution.py:530
  217.2 4.0 %collective-permute-done.22.refs_7_ = bf16[128,2048]{1,0:T(8,128)(2,1)S(1)} collective-permute-done((bf16[128,2048]{1,0:T(8,128)(2,1)S(1)}, bf16[128,2048]{1,0:T(8,128)(2,1)S(1)}, u32[]{:S(2)}, u32[]{:S(2)}) %collective-permute-start.22) | collective-permute-done | bytes 524320 | tf_op jit(solution)/shard_map/ppermute | solution.py:533
  221.2 16.9 %gated.1.hidden = bf16[1024,1408]{1,0:T(8,128)(2,1)S(1)} custom-call(s32[4]{0:T(128)S(1)} %pad_add_fusion.place.refs_0_, f32[8,1408]{1,0:T(8,128)S(1)} %get-tuple-element.33.refs_1_, f32[8,1408]{1,0:T(8,128)S(1)} %collective-permute-done.refs_2_, bf16[256,2048]{1,0:T(8,128)(2,1)S(1)} %get-tuple-element.39.refs_3_, ...), custom_call_target="tpu_custom_call" | custom-call | flops 12000000000 | bytes 20000000 | tf_op jit(solution)/shard_map/gated/pallas_call | solution.py:401
  238.2 2.6 keep.7
  244.4 2.6 keep.6
  250.5 2.9 keep.5
  261.3 2.8 collective-permute-start.49
  264.1 2.6 keep.4
  268.2 2.7 collective-permute-start.43
  272.6 2.8 collective-permute-start.44
  275.6 3.0 %collective-permute-done.48.second = bf16[256,512]{1,0:T(8,128)(2,1)S(1)} collective-permute-done((bf16[256,512]{1,0:T(8,128)(2,1)S(1)}, bf16[256,512]{1,0:T(8,128)(2,1)S(1)}, u32[]{:S(2)}, u32[]{:S(2)}) %collective-permute-start.48) | collective-permute-done | bytes 262176 | tf_op jit(solution)/shard_map/ppermute | solution.py:533
  279.6 4.3 %collective-permute-done.42.first = bf16[256,512]{1,0:T(8,128)(2,1)S(1)} collective-permute-done((bf16[256,512]{1,0:T(8,128)(2,1)S(1)}, bf16[256,512]{1,0:T(8,128)(2,1)S(1)}, u32[]{:S(2)}, u32[]{:S(2)}) %collective-permute-start.42) | collective-permute-done | bytes 262176 | tf_op jit(solution)/shard_map/ppermute | solution.py:530
  283.9 4.4 %collective-permute-done.43.second = bf16[256,512]{1,0:T(8,128)(2,1)S(1)} collective-permute-done((bf16[256,512]{1,0:T(8,128)(2,1)S(1)}, bf16[256,512]{1,0:T(8,128)(2,1)S(1)}, u32[]{:S(2)}, u32[]{:S(2)}) %collective-permute-start.43) | collective-permute-done | bytes 262176 | tf_op jit(solution)/shard_map/ppermute | solution.py:533
  (145 shorter events, 69.2 us)
Async XLA Ops:
  1.4 21.1 %collective-permute-start.6 = (bf16[2,128,512]{2,1,0:T(8,128)(2,1)S(1)}, bf16[2,128,512]{2,1,0:T(8,128)(2,1)S(1)}, u32[]{:S(2)}, u32[]{:S(2)}) collective-permute-start(bf16[2,128,512]{2,1,0:T(8,128)(2,1)S(1)} %fusion), channel_id=1, source_target_pairs={{0,4},{2,6},{4,8},{6,10},{8,12},{10,14},{12,0},{14,2},{1,5},{3,7},... | collective-permute-start | bytes 786440 | tf_op jit(solution)/shard_map/ppermute | solution.py:542
  4.5 21.3 %collective-permute-start.14 = (bf16[2,128,512]{2,1,0:T(8,128)(2,1)S(1)}, bf16[2,128,512]{2,1,0:T(8,128)(2,1)S(1)}, u32[]{:S(2)}, u32[]{:S(2)}) collective-permute-start(bf16[2,128,512]{2,1,0:T(8,128)(2,1)S(1)} %fusion), channel_id=1, source_target_pairs={{0,12},{2,14},{4,0},{6,2},{8,4},{10,6},{12,8},{14,10},{1,13},{3,15... | collective-permute-start | bytes 786440 | tf_op jit(solution)/shard_map/ppermute | solution.py:542
  23.8 32.2 %collective-permute-start.5 = (bf16[2,256,512]{2,1,0:T(8,128)(2,1)S(1)}, bf16[2,256,512]{2,1,0:T(8,128)(2,1)S(1)}, u32[]{:S(2)}, u32[]{:S(2)}) collective-permute-start(bf16[2,256,512]{2,1,0:T(8,128)(2,1)S(1)} %pad_maximum_fusion.1.refs_9_), channel_id=1, source_target_pairs={{0,2},{2,0},{4,6},{6,4},{8,10},{10,8},{12,14},{14,12},{1,3},{3,1},... | collective-permute-start | bytes 1572872 | tf_op jit(solution)/shard_map/ppermute | solution.py:533
  25.1 22.5 %collective-permute-start.8 = (bf16[2,128,512]{2,1,0:T(8,128)(2,1)S(1)}, bf16[2,128,512]{2,1,0:T(8,128)(2,1)S(1)}, u32[]{:S(2)}, u32[]{:S(2)}) collective-permute-start(bf16[2,128,512]{2,1,0:T(8,128)(2,1)S(1)} %collective-permute-done.6.refs_11_), channel_id=1, source_target_pairs={{0,2},{2,0},{4,6},{6,4},{8,10},{10,8},{12,14},{14,12},{1,3},{3,1},... | collective-permute-start | bytes 786440 | tf_op jit(solution)/shard_map/ppermute | solution.py:533
  25.8 27.5 %collective-permute-start.16 = (bf16[2,128,512]{2,1,0:T(8,128)(2,1)S(1)}, bf16[2,128,512]{2,1,0:T(8,128)(2,1)S(1)}, u32[]{:S(2)}, u32[]{:S(2)}) collective-permute-start(bf16[2,128,512]{2,1,0:T(8,128)(2,1)S(1)} %collective-permute-done.14.refs_19_), channel_id=1, source_target_pairs={{0,2},{2,0},{4,6},{6,4},{8,10},{10,8},{12,14},{14,12},{1,3},{3,1},... | collective-permute-start | bytes 786440 | tf_op jit(solution)/shard_map/ppermute | solution.py:533
  30.8 23.1 %collective-permute-start.7 = (bf16[2,128,512]{2,1,0:T(8,128)(2,1)S(1)}, bf16[2,128,512]{2,1,0:T(8,128)(2,1)S(1)}, u32[]{:S(2)}, u32[]{:S(2)}) collective-permute-start(bf16[2,128,512]{2,1,0:T(8,128)(2,1)S(1)} %collective-permute-done.6.refs_11_), channel_id=1, source_target_pairs={{0,16},{16,0},{1,17},{17,1},{2,18},{18,2},{3,19},{19,3},{4,20},{20... | collective-permute-start | bytes 786440 | tf_op jit(solution)/shard_map/ppermute | solution.py:530
  32.3 23.1 %collective-permute-start.15 = (bf16[2,128,512]{2,1,0:T(8,128)(2,1)S(1)}, bf16[2,128,512]{2,1,0:T(8,128)(2,1)S(1)}, u32[]{:S(2)}, u32[]{:S(2)}) collective-permute-start(bf16[2,128,512]{2,1,0:T(8,128)(2,1)S(1)} %collective-permute-done.14.refs_19_), channel_id=1, source_target_pairs={{0,16},{16,0},{1,17},{17,1},{2,18},{18,2},{3,19},{19,3},{4,20},{20... | collective-permute-start | bytes 786440 | tf_op jit(solution)/shard_map/ppermute | solution.py:530
  53.3 28.2 %collective-permute-start.24 = (bf16[256,1408]{1,0:T(8,128)(2,1)S(1)}, bf16[256,1408]{1,0:T(8,128)(2,1)S(1)}, u32[]{:S(2)}, u32[]{:S(2)}) collective-permute-start(bf16[256,1408]{1,0:T(8,128)(2,1)S(1)} %get-tuple-element.41), channel_id=1, source_target_pairs={{0,2},{2,0},{4,6},{6,4},{8,10},{10,8},{12,14},{14,12},{1,3},{3,1},... | collective-permute-start | bytes 2162696 | tf_op jit(solution)/shard_map/ppermute | solution.py:533
  63.1 20.8 %collective-permute-start.26 = (bf16[256,1408]{1,0:T(8,128)(2,1)S(1)}, bf16[256,1408]{1,0:T(8,128)(2,1)S(1)}, u32[]{:S(2)}, u32[]{:S(2)}) collective-permute-start(bf16[256,1408]{1,0:T(8,128)(2,1)S(1)} %get-tuple-element.40.refs_8_), channel_id=1, source_target_pairs={{0,4},{2,6},{4,8},{6,10},{8,12},{10,14},{12,0},{14,2},{1,5},{3,7},... | collective-permute-start | bytes 2162696 | tf_op jit(solution)/shard_map/ppermute | solution.py:542
  68.7 20.7 %collective-permute-start.23 = (bf16[256,1408]{1,0:T(8,128)(2,1)S(1)}, bf16[256,1408]{1,0:T(8,128)(2,1)S(1)}, u32[]{:S(2)}, u32[]{:S(2)}) collective-permute-start(bf16[256,1408]{1,0:T(8,128)(2,1)S(1)} %get-tuple-element.40.refs_8_), channel_id=1, source_target_pairs={{0,1},{1,0},{2,3},{3,2},{4,5},{5,4},{6,7},{7,6},{8,9},{9,8},{10,11... | collective-permute-start | bytes 2162696 | tf_op jit(solution)/shard_map/ppermute | solution.py:539
  72.3 27.1 %collective-permute-start.56 = (bf16[2,704,256]{2,1,0:T(8,128)(2,1)S(1)}, bf16[2,704,256]{2,1,0:T(8,128)(2,1)S(1)}, u32[]{:S(2)}, u32[]{:S(2)}) collective-permute-start(bf16[2,704,256]{2,1,0:T(8,128)(2,1)S(1)} %pad_maximum_fusion.refs_0_), channel_id=1, source_target_pairs={{0,12},{2,14},{4,0},{6,2},{8,4},{10,6},{12,8},{14,10},{1,13},{3,15... | collective-permute-start | bytes 2162696 | tf_op jit(solution)/shard_map/ppermute | solution.py:542
  75.7 39.2 %collective-permute-start.39 = (bf16[2,704,256]{2,1,0:T(8,128)(2,1)S(1)}, bf16[2,704,256]{2,1,0:T(8,128)(2,1)S(1)}, u32[]{:S(2)}, u32[]{:S(2)}) collective-permute-start(bf16[2,704,256]{2,1,0:T(8,128)(2,1)S(1)} %pad_maximum_fusion.refs_0_), channel_id=1, source_target_pairs={{0,4},{2,6},{4,8},{6,10},{8,12},{10,14},{12,0},{14,2},{1,5},{3,7},... | collective-permute-start | bytes 2162696 | tf_op jit(solution)/shard_map/ppermute | solution.py:542
  81.5 64.3 %collective-permute-start.18 = (bf16[256,2048]{1,0:T(8,128)(2,1)S(1)}, bf16[256,2048]{1,0:T(8,128)(2,1)S(1)}, u32[]{:S(2)}, u32[]{:S(2)}) collective-permute-start(bf16[256,2048]{1,0:T(8,128)(2,1)S(1)} %get-tuple-element.37), channel_id=1, source_target_pairs={{0,1},{1,0},{2,3},{3,2},{4,5},{5,4},{6,7},{7,6},{8,9},{9,8},{10,11... | collective-permute-start | bytes 3145736 | tf_op jit(solution)/shard_map/ppermute | solution.py:539
  83.9 46.4 %collective-permute-start.28 = (bf16[256,1408]{1,0:T(8,128)(2,1)S(1)}, bf16[256,1408]{1,0:T(8,128)(2,1)S(1)}, u32[]{:S(2)}, u32[]{:S(2)}) collective-permute-start(bf16[256,1408]{1,0:T(8,128)(2,1)S(1)} %collective-permute-done.24.refs_10_), channel_id=1, source_target_pairs={{0,4},{2,6},{4,8},{6,10},{8,12},{10,14},{12,0},{14,2},{1,5},{3,7},... | collective-permute-start | bytes 2162696 | tf_op jit(solution)/shard_map/ppermute | solution.py:542
  89.4 56.4 %collective-permute-start.30 = (bf16[256,1408]{1,0:T(8,128)(2,1)S(1)}, bf16[256,1408]{1,0:T(8,128)(2,1)S(1)}, u32[]{:S(2)}, u32[]{:S(2)}) collective-permute-start(bf16[256,1408]{1,0:T(8,128)(2,1)S(1)} %collective-permute-done.26.refs_12_), channel_id=1, source_target_pairs={{0,4},{2,6},{4,8},{6,10},{8,12},{10,14},{12,0},{14,2},{1,5},{3,7},... | collective-permute-start | bytes 2162696 | tf_op jit(solution)/shard_map/ppermute | solution.py:542
  99.4 48.0 %collective-permute-start.25 = (bf16[256,1408]{1,0:T(8,128)(2,1)S(1)}, bf16[256,1408]{1,0:T(8,128)(2,1)S(1)}, u32[]{:S(2)}, u32[]{:S(2)}) collective-permute-start(bf16[256,1408]{1,0:T(8,128)(2,1)S(1)} %collective-permute-done.24.refs_10_), channel_id=1, source_target_pairs={{0,1},{1,0},{2,3},{3,2},{4,5},{5,4},{6,7},{7,6},{8,9},{9,8},{10,11... | collective-permute-start | bytes 2162696 | tf_op jit(solution)/shard_map/ppermute | solution.py:539
  114.8 32.6 %collective-permute-start.27 = (bf16[256,1408]{1,0:T(8,128)(2,1)S(1)}, bf16[256,1408]{1,0:T(8,128)(2,1)S(1)}, u32[]{:S(2)}, u32[]{:S(2)}) collective-permute-start(bf16[256,1408]{1,0:T(8,128)(2,1)S(1)} %collective-permute-done.26.refs_12_), channel_id=1, source_target_pairs={{0,1},{1,0},{2,3},{3,2},{4,5},{5,4},{6,7},{7,6},{8,9},{9,8},{10,11... | collective-permute-start | bytes 2162696 | tf_op jit(solution)/shard_map/ppermute | solution.py:539
  130.3 30.9 %collective-permute-start.32 = (bf16[256,1408]{1,0:T(8,128)(2,1)S(1)}, bf16[256,1408]{1,0:T(8,128)(2,1)S(1)}, u32[]{:S(2)}, u32[]{:S(2)}) collective-permute-start(bf16[256,1408]{1,0:T(8,128)(2,1)S(1)} %collective-permute-done.28.refs_14_), channel_id=1, source_target_pairs={{0,4},{2,6},{4,8},{6,10},{8,12},{10,14},{12,0},{14,2},{1,5},{3,7},... | collective-permute-start | bytes 2162696 | tf_op jit(solution)/shard_map/ppermute | solution.py:542
  145.7 30.9 %collective-permute-start.40 = (bf16[2,704,256]{2,1,0:T(8,128)(2,1)S(1)}, bf16[2,704,256]{2,1,0:T(8,128)(2,1)S(1)}, u32[]{:S(2)}, u32[]{:S(2)}) collective-permute-start(bf16[2,704,256]{2,1,0:T(8,128)(2,1)S(1)} %collective-permute-done.39.refs_0_), channel_id=1, source_target_pairs={{0,4},{2,6},{4,8},{6,10},{8,12},{10,14},{12,0},{14,2},{1,5},{3,7},... | collective-permute-start | bytes 2162696 | tf_op jit(solution)/shard_map/ppermute | solution.py:542
  145.7 46.3 %collective-permute-start.34 = (bf16[256,1408]{1,0:T(8,128)(2,1)S(1)}, bf16[256,1408]{1,0:T(8,128)(2,1)S(1)}, u32[]{:S(2)}, u32[]{:S(2)}) collective-permute-start(bf16[256,1408]{1,0:T(8,128)(2,1)S(1)} %collective-permute-done.30.refs_16_), channel_id=1, source_target_pairs={{0,4},{2,6},{4,8},{6,10},{8,12},{10,14},{12,0},{14,2},{1,5},{3,7},... | collective-permute-start | bytes 2162696 | tf_op jit(solution)/shard_map/ppermute | solution.py:542
  147.4 54.8 %collective-permute-start.20 = (bf16[256,2048]{1,0:T(8,128)(2,1)S(1)}, bf16[256,2048]{1,0:T(8,128)(2,1)S(1)}, u32[]{:S(2)}, u32[]{:S(2)}) collective-permute-start(bf16[256,2048]{1,0:T(8,128)(2,1)S(1)} %get-tuple-element.39.refs_3_), channel_id=1, source_target_pairs={{0,2},{2,0},{4,6},{6,4},{8,10},{10,8},{12,14},{14,12},{1,3},{3,1},... | collective-permute-start | bytes 3145736 | tf_op jit(solution)/shard_map/ppermute | solution.py:533
  147.5 55.2 %collective-permute-start.19 = (bf16[256,2048]{1,0:T(8,128)(2,1)S(1)}, bf16[256,2048]{1,0:T(8,128)(2,1)S(1)}, u32[]{:S(2)}, u32[]{:S(2)}) collective-permute-start(bf16[256,2048]{1,0:T(8,128)(2,1)S(1)} %get-tuple-element.39.refs_3_), channel_id=1, source_target_pairs={{0,16},{16,0},{1,17},{17,1},{2,18},{18,2},{3,19},{19,3},{4,20},{20... | collective-permute-start | bytes 3145736 | tf_op jit(solution)/shard_map/ppermute | solution.py:530
  161.2 41.0 %collective-permute-start.36 = (bf16[256,1408]{1,0:T(8,128)(2,1)S(1)}, bf16[256,1408]{1,0:T(8,128)(2,1)S(1)}, u32[]{:S(2)}, u32[]{:S(2)}) collective-permute-start(bf16[256,1408]{1,0:T(8,128)(2,1)S(1)} %collective-permute-done.32.refs_18_), channel_id=1, source_target_pairs={{0,4},{2,6},{4,8},{6,10},{8,12},{10,14},{12,0},{14,2},{1,5},{3,7},... | collective-permute-start | bytes 2162696 | tf_op jit(solution)/shard_map/ppermute | solution.py:542
  176.6 26.2 %collective-permute-start.29 = (bf16[256,1408]{1,0:T(8,128)(2,1)S(1)}, bf16[256,1408]{1,0:T(8,128)(2,1)S(1)}, u32[]{:S(2)}, u32[]{:S(2)}) collective-permute-start(bf16[256,1408]{1,0:T(8,128)(2,1)S(1)} %collective-permute-done.28.refs_14_), channel_id=1, source_target_pairs={{0,1},{1,0},{2,3},{3,2},{4,5},{5,4},{6,7},{7,6},{8,9},{9,8},{10,11... | collective-permute-start | bytes 2162696 | tf_op jit(solution)/shard_map/ppermute | solution.py:539
  209.0 38.0 %collective-permute-start.46 = (bf16[2,704,256]{2,1,0:T(8,128)(2,1)S(1)}, bf16[2,704,256]{2,1,0:T(8,128)(2,1)S(1)}, u32[]{:S(2)}, u32[]{:S(2)}) collective-permute-start(bf16[2,704,256]{2,1,0:T(8,128)(2,1)S(1)} %pad_maximum_fusion.refs_0_), channel_id=1, source_target_pairs={{0,1},{1,0},{2,3},{3,2},{4,5},{5,4},{6,7},{7,6},{8,9},{9,8},{10,11... | collective-permute-start | bytes 2162696 | tf_op jit(solution)/shard_map/ppermute | solution.py:539
  209.0 35.3 %collective-permute-start.51 = (bf16[2,704,256]{2,1,0:T(8,128)(2,1)S(1)}, bf16[2,704,256]{2,1,0:T(8,128)(2,1)S(1)}, u32[]{:S(2)}, u32[]{:S(2)}) collective-permute-start(bf16[2,704,256]{2,1,0:T(8,128)(2,1)S(1)} %collective-permute-done.39.refs_0_), channel_id=1, source_target_pairs={{0,1},{1,0},{2,3},{3,2},{4,5},{5,4},{6,7},{7,6},{8,9},{9,8},{10,11... | collective-permute-start | bytes 2162696 | tf_op jit(solution)/shard_map/ppermute | solution.py:539
  209.5 28.7 %collective-permute-start.57 = (bf16[2,704,256]{2,1,0:T(8,128)(2,1)S(1)}, bf16[2,704,256]{2,1,0:T(8,128)(2,1)S(1)}, u32[]{:S(2)}, u32[]{:S(2)}) collective-permute-start(bf16[2,704,256]{2,1,0:T(8,128)(2,1)S(1)} %collective-permute-done.56.refs_0_), channel_id=1, source_target_pairs={{0,1},{1,0},{2,3},{3,2},{4,5},{5,4},{6,7},{7,6},{8,9},{9,8},{10,11... | collective-permute-start | bytes 2162696 | tf_op jit(solution)/shard_map/ppermute | solution.py:539
  217.2 31.5 %collective-permute-start.41 = (bf16[2,704,256]{2,1,0:T(8,128)(2,1)S(1)}, bf16[2,704,256]{2,1,0:T(8,128)(2,1)S(1)}, u32[]{:S(2)}, u32[]{:S(2)}) collective-permute-start(bf16[2,704,256]{2,1,0:T(8,128)(2,1)S(1)} %collective-permute-done.40.refs_0_), channel_id=1, source_target_pairs={{0,1},{1,0},{2,3},{3,2},{4,5},{5,4},{6,7},{7,6},{8,9},{9,8},{10,11... | collective-permute-start | bytes 2162696 | tf_op jit(solution)/shard_map/ppermute | solution.py:539
  248.7 18.6 %collective-permute-start.53 = (bf16[256,512]{1,0:T(8,128)(2,1)S(1)}, bf16[256,512]{1,0:T(8,128)(2,1)S(1)}, u32[]{:S(2)}, u32[]{:S(2)}) collective-permute-start(bf16[256,512]{1,0:T(8,128)(2,1)S(1)} %get-tuple-element.55), channel_id=1, source_target_pairs={{0,2},{2,0},{4,6},{6,4},{8,10},{10,8},{12,14},{14,12},{1,3},{3,1},... | collective-permute-start | bytes 786440 | tf_op jit(solution)/shard_map/ppermute | solution.py:533
  256.9 21.7 %collective-permute-start.48 = (bf16[256,512]{1,0:T(8,128)(2,1)S(1)}, bf16[256,512]{1,0:T(8,128)(2,1)S(1)}, u32[]{:S(2)}, u32[]{:S(2)}) collective-permute-start(bf16[256,512]{1,0:T(8,128)(2,1)S(1)} %get-tuple-element.51), channel_id=1, source_target_pairs={{0,2},{2,0},{4,6},{6,4},{8,10},{10,8},{12,14},{14,12},{1,3},{3,1},... | collective-permute-start | bytes 786440 | tf_op jit(solution)/shard_map/ppermute | solution.py:533
  261.3 18.1 %collective-permute-start.49 = (bf16[256,512]{1,0:T(8,128)(2,1)S(1)}, bf16[256,512]{1,0:T(8,128)(2,1)S(1)}, u32[]{:S(2)}, u32[]{:S(2)}) collective-permute-start(bf16[256,512]{1,0:T(8,128)(2,1)S(1)} %get-tuple-element.52), channel_id=1, source_target_pairs={{0,18},{2,16},{4,22},{6,20},{8,26},{10,24},{12,30},{14,28},{16,2},... | collective-permute-start | bytes 786440 | tf_op jit(solution)/shard_map/ppermute | solution.py:536
  268.2 20.1 %collective-permute-start.43 = (bf16[256,512]{1,0:T(8,128)(2,1)S(1)}, bf16[256,512]{1,0:T(8,128)(2,1)S(1)}, u32[]{:S(2)}, u32[]{:S(2)}) collective-permute-start(bf16[256,512]{1,0:T(8,128)(2,1)S(1)} %get-tuple-element.47), channel_id=1, source_target_pairs={{0,2},{2,0},{4,6},{6,4},{8,10},{10,8},{12,14},{14,12},{1,3},{3,1},... | collective-permute-start | bytes 786440 | tf_op jit(solution)/shard_map/ppermute | solution.py:533
  (43 other events, 561.4 us)

commit v2 on v1

--- a/solution.py
+++ b/solution.py
@@ -94,13 +94,15 @@
     return pieces
 
 
-def pack_kernel(place, gate, up, gate_scale, up_scale, kept, sent, scale):
-    keep = kept.shape[1] // 2
-
-    def put(out, gates, ups):
+def pack_kernel(place, gate, up, gate_scale, up_scale, kept, kept_late, sent, sent_late, scale):
+    keep = scale.shape[1] // 2
+    cut = kept.shape[1]
+
+    def put(outs, gates, ups):
         at = 0
         for piece in packed_pair(gates, ups, keep):
-            out[:, at : at + piece.shape[1]] = piece.astype(out.dtype)
+            out, to = (outs[1], at - cut) if at >= cut and len(outs) > 1 else (outs[0], at)
+            out[:, to : to + piece.shape[1]] = piece.astype(out.dtype)
             at += piece.shape[1]
 
     low = (gate[...], up[...])
@@ -110,15 +112,15 @@
 
     @pl.when(place[1] == 0)
     def _():
-        put(kept, *low)
-        put(sent, *high)
-        put(scale, *scales)
+        put((kept, kept_late), *low)
+        put((sent, sent_late), *high)
+        put((scale,), *scales)
 
     @pl.when(place[1] != 0)
     def _():
-        put(kept, *high)
-        put(sent, *low)
-        put(scale, *high_scales)
+        put((kept, kept_late), *high)
+        put((sent, sent_late), *low)
+        put((scale,), *high_scales)
 
 
 def run_pack(place, gate, up, gate_scale, up_scale):
@@ -127,17 +129,18 @@
     block = min(rows, 64)
     weight = pl.BlockSpec((block, both), lambda i, p: (i, p[0]))
     scale = pl.BlockSpec((1, both), lambda i, p: (0, p[0]))
-    out = pl.BlockSpec((block, both), lambda i, p: (i, 0))
-    shape = jax.ShapeDtypeStruct((rows, both), BF)
+    cut = (both // 256 + 1) // 2 * 256
+    outs = [pl.BlockSpec((block, c), lambda i, p: (i, 0)) for c in (cut, both - cut)] * 2
+    shapes = [jax.ShapeDtypeStruct((rows, c), BF) for c in (cut, both - cut)] * 2
     return pl.pallas_call(
         pack_kernel,
         grid_spec=pltpu.PrefetchScalarGridSpec(
             num_scalar_prefetch=1,
             grid=(rows // block,),
             in_specs=[weight, weight, scale, scale],
-            out_specs=(out, out, pl.BlockSpec((8, both), lambda i, p: (0, 0))),
+            out_specs=(*outs, pl.BlockSpec((8, both), lambda i, p: (0, 0))),
         ),
-        out_shape=(shape, shape, jax.ShapeDtypeStruct((8, both), F32)),
+        out_shape=(*shapes, jax.ShapeDtypeStruct((8, both), F32)),
         compiler_params=room(12),
         name="pack",
         cost_estimate=pl.CostEstimate(flops=3_000_000_000, bytes_accessed=5_000_000, transcendentals=0),
@@ -335,11 +338,15 @@
     )(place, tokens, part, other, gain)
 
 
-def gated_kernel(n_rows, starts, n_weights, *refs):
+def gated_kernel(offset, n_rows, starts, n_weights, *refs):
     place, scale, other_scale = refs[:3]
     rows = refs[3 : 3 + n_rows]
     parts = refs[3 + n_rows : 3 + n_rows + n_weights]
-    hidden, weights, stage, row_sems, sems = refs[3 + n_rows + n_weights :]
+    if starts:
+        hidden, stage, weights, row_sems, sems = refs[3 + n_rows + n_weights :]
+    else:
+        hidden, weights, row_sems, sems = refs[3 + n_rows + n_weights :]
+        stage = rows[0]
     shard, both = parts[0].shape
     keep = both // 2
     aligned = keep // 128 * 128
@@ -374,7 +381,7 @@
         for copy in batches[j]:
             copy.wait()
         for at in range(0, aligned, 128):
-            sums = product(2 * (j * aligned + at), 256) * line[0:1, 2 * at : 2 * at + 256]
+            sums = product(2 * (j * aligned + at), 256) * line[0:1, offset + 2 * at : offset + 2 * at + 256]
             gate, up = sums[:, :128], sums[:, 128:]
             hidden[:, j * aligned + at : j * aligned + at + 128] = (jax.nn.silu(gate) * up).astype(BF)
     if tail:
@@ -382,7 +389,7 @@
             copy.wait()
         sums = product(4 * aligned, 4 * tail)
         own, other = (
-            sums[:, 2 * j * tail : 2 * (j + 1) * tail] * line[0:1, 2 * aligned :]
+            sums[:, 2 * j * tail : 2 * (j + 1) * tail] * line[0:1, offset + 2 * aligned :]
             for j, line in enumerate((scale, other_scale))
         )
         lane = lax.broadcasted_iota(jnp.int32, own.shape, 1)
@@ -391,36 +398,40 @@
         hidden[:, 2 * aligned :] = (jax.nn.silu(gate) * up).astype(BF)
 
 
-def run_gated(place, scale, other_scale, rows, parts):
+def run_gated(place, scale, other_scale, rows, parts, offset):
     starts, total = [], 0
     for r in rows:
         starts.append(total)
         total += r.shape[0]
+    gathers = len(rows) > 1
     width = rows[0].shape[1]
     both = parts[0].shape[1]
-    return pl.pallas_call(
-        functools.partial(gated_kernel, len(rows), tuple(starts), len(parts)),
-        out_shape=jax.ShapeDtypeStruct((total, both), BF),
-        in_specs=[SMEM, VMEM, VMEM] + [HBM] * (len(rows) + len(parts)),
-        out_specs=VMEM,
+    shapes = [jax.ShapeDtypeStruct((total, both), BF), jax.ShapeDtypeStruct((total, width), BF)]
+    return pl.pallas_call(
+        functools.partial(
+            gated_kernel, offset, len(rows), tuple(starts) if gathers else (), len(parts)
+        ),
+        out_shape=tuple(shapes) if gathers else shapes[0],
+        in_specs=[SMEM, VMEM, VMEM] + [HBM if gathers else VMEM] * len(rows) + [HBM] * len(parts),
+        out_specs=(VMEM, VMEM) if gathers else VMEM,
         scratch_shapes=[
             pltpu.VMEM((width, 2 * both), BF),
-            pltpu.VMEM((total, width), BF),
             pltpu.SemaphoreType.DMA((len(rows),)),
             pltpu.SemaphoreType.DMA((2 * len(parts),)),
         ],
-        compiler_params=room(34),
+        compiler_params=room(24),
         name="gated",
-        cost_estimate=pl.CostEstimate(flops=12_000_000_000, bytes_accessed=20_000_000, transcendentals=1_500_000),
+        cost_estimate=pl.CostEstimate(flops=6_000_000_000, bytes_accessed=12_000_000, transcendentals=700_000),
     )(place, scale, other_scale, *rows, *parts)
 
 
-def keep_kernel(k, place, hidden, scale, middle, *refs):
+def keep_kernel(k, place, early, late, scale, middle, *refs):
     both, both_other, base = refs[:3]
     outs, ends = refs[3:6], refs[6]
     _, keep, width = both.shape
     aligned = keep // 128 * 128
     tail = keep - aligned
+    cut = early.shape[1] // 2
     rows = base.shape[0]
     for i in range(2):
         own, other = both.at[i], both_other.at[i]
@@ -429,31 +440,35 @@
         from_lanes = pl.ds(pl.multiple_of((2 * k + y) * width, width), width)
         ends[:tail, :] = own[aligned:, :]
         ends[tail:, :] = other[aligned:, :]
-        total = jnp.dot(hidden[:, :aligned], own[:aligned, :], preferred_element_type=F32)
-        total += jnp.dot(
-            hidden[:, aligned : 2 * aligned], other[:aligned, :], preferred_element_type=F32
-        )
-        total += jnp.dot(hidden[:, 2 * aligned :], ends[...], preferred_element_type=F32)
+        total = jnp.dot(late[:, 2 * (aligned - cut) :], ends[...], preferred_element_type=F32)
+        for j, weight in enumerate((own, other)):
+            total += jnp.dot(
+                early[:, j * cut : (j + 1) * cut], weight[:cut, :], preferred_element_type=F32
+            )
+            total += jnp.dot(
+                late[:, j * (aligned - cut) : (j + 1) * (aligned - cut)], weight[cut:aligned, :],
+                preferred_element_type=F32,
+            )
         total = total * scale[i, 1:2, :]
         base[:, lanes] = total[:rows, :] + middle[:, from_lanes].astype(F32)
         for j, out in enumerate(outs):
             out[:, lanes] = total[(j + 1) * rows : (j + 2) * rows, :].astype(BF)
 
 
-def run_keep(place, hidden, scale, middle, parts, k):
-    rows = hidden.shape[0] // 4
+def run_keep(place, early, late, scale, middle, parts, k):
+    rows = early.shape[0] // 4
     _, keep, width = parts[0].shape
     shape = jax.ShapeDtypeStruct((rows, 2 * width), BF)
     return pl.pallas_call(
         functools.partial(keep_kernel, k),
-        in_specs=[SMEM] + [VMEM] * 5,
+        in_specs=[SMEM] + [VMEM] * 6,
         out_specs=(VMEM, VMEM, VMEM, VMEM),
         scratch_shapes=[pltpu.VMEM((2 * (keep % 128), width), BF)],
         out_shape=(jax.ShapeDtypeStruct(shape.shape, F32), shape, shape, shape),
         compiler_params=room(20),
         name="keep",
         cost_estimate=pl.CostEstimate(flops=2_000_000_000, bytes_accessed=5_000_000, transcendentals=0),
-    )(place, hidden, scale, middle, *parts)
+    )(place, early, late, scale, middle, *parts)
 
 
 def join_kernel(base, first, second, third, out):
@@ -559,7 +574,9 @@
 
     own_scale = jnp.stack([output_scale, down_scale])
     pair = jnp.stack([own_scale, beside(own_scale)])
-    scales = [pair] + [around(pair, k) for k in range(1, n_ring)]
+    scales = [pair]
+    for _ in range(1, n_ring):
+        scales.append(around(scales[-1]))
 
     def circled(start, back):
         chain = [start, around(start)]
@@ -569,9 +586,13 @@
             chain.append(around(start, -1))
         return [(c, partner(c)) for c in chain]
 
-    gated_kept, gated_sent, gated_scale = run_pack(place, gate_weight, up_weight, gate_scale[None], up_scale[None])
-    own_column, next_column = circled(gated_kept, 0), circled(beside(gated_sent), 0)
-    gated_parts = [a + b for a, b in zip(own_column, next_column)]
+    kept, kept_late, sent, sent_late, gated_scale = run_pack(
+        place, gate_weight, up_weight, gate_scale[None], up_scale[None]
+    )
+    gated_parts = [
+        sum((a + b for a, b in zip(circled(first, 0), circled(beside(second), 0))), ())
+        for first, second in ((kept, sent), (kept_late, sent_late))
+    ]
     down_kept, down_sent = run_turn(place, down_weight)
     down_parts = circled(jnp.stack([down_kept, beside(down_sent)]), 1)
 
@@ -585,22 +606,21 @@
     ax, ay = across(here), beside(here)
     cut = rows // 2
     far = [across(ay[:cut]), beside(ax[cut:])]
-    hidden = run_gated(
-        place, gated_scale, partner(gated_scale), [here, ax, ay] + far,
-        sum(gated_parts, ()),
-    )
+    other_scale = partner(gated_scale)
+    early, gathered = run_gated(place, gated_scale, other_scale, [here, ax, ay] + far, gated_parts[0], 0)
+    late = run_gated(place, gated_scale, other_scale, [gathered], gated_parts[1], kept.shape[1])
 
     pieces = []
     steps = (0, 1) + tuple(range(n_ring - 1, 1, -1))
     for k in steps:
-        base, to_x, to_y, to_far = run_keep(place, hidden, scales[k], middle_mine, down_parts[k], k)
+        base, to_x, to_y, to_far = run_keep(place, early, late, scales[k], middle_mine, down_parts[k], k)
         total = run_join(
             base, across(to_x), beside(to_y),
             corner(to_far),
         )
         pieces.append((total, partner(total)))
-    early = run_collect(place, n_ring, steps[:-1], sum(pieces[:-1], ()))
-    return run_collect(place, n_ring, steps[-1:], pieces[-1], early)
+    most = run_collect(place, n_ring, steps[:-1], sum(pieces[:-1], ()))
+    return run_collect(place, n_ring, steps[-1:], pieces[-1], most)
 
 
 def solution(mesh):

time: 294 us -> 284 us (0.966)
  starting transfers between devices: 65.2 us -> 58.6 us
  waiting for transfers between devices: 180 us -> 174 us
  Pallas kernels: 42.4 us -> 45.7 us
    ppermute x13 -> x14, starting transfers between devices: 21.4 us -> 12.9 us  [beside(): return lax.ppermute(value, 'fs', col_swap)]
    ppermute x18 -> x26, waiting for transfers between devices: 0.05 us -> 4.52 us  [partner(): return lax.ppermute(value, 'tp', swap)]
    ppermute x12, waiting for transfers between devices: 25.6 us -> 21.7 us  [across(): return lax.ppermute(value, 'rep', swap)]
    pallas_call x1 -> x2, Pallas kernels: 16.9 us -> 20.4 us  [run_gated(): pl.pallas_call(functools.partial(gated_kernel, offset, len(rows), tuple(s...]
    ppermute x12, starting transfers between devices: 13.4 us -> 10.3 us  [across(): return lax.ppermute(value, 'rep', swap)]
    ppermute x13 -> x14, waiting for transfers between devices: 39.4 us -> 37 us  [beside(): return lax.ppermute(value, 'fs', col_swap)]
    ppermute x15 -> x21, starting transfers between devices: 23.1 us -> 25.4 us  [around(): lax.ppermute(value, 'fs', [(i, (i + 2 * steps) % n_fs) for i in range(n_f...]
    ppermute x15 -> x21, waiting for transfers between devices: 112 us -> 111 us  [around(): lax.ppermute(value, 'fs', [(i, (i + 2 * steps) % n_fs) for i in range(n_f...]
  transfers between devices with their start and end apart: 62 -> 77, of which waited for: 29 -> 32; matrix products, arithmetic and copies ran while one was open for 0% -> 0% of each run, Pallas kernels for 14% -> 16%
where the time goes in v2:
time: 284 us
  waiting for transfers between devices  174 us (61%)
  starting transfers between devices  58.6 us (21%)
  Pallas kernels  45.7 us (16%)
  local copies, waits for them, and re-layouts  3.78 us (1%)
    ppermute x21, waiting for transfers between devices, around(): lax.ppermute(value, 'fs', [(i, (i + 2 * steps) % n_fs) for i in range(n_f...  111 us
    ppermute x14, waiting for transfers between devices, beside(): return lax.ppermute(value, 'fs', col_swap)  37 us
    ppermute x21, starting transfers between devices, around(): lax.ppermute(value, 'fs', [(i, (i + 2 * steps) % n_fs) for i in range(n_f...  25.4 us
    ppermute x12, waiting for transfers between devices, across(): return lax.ppermute(value, 'rep', swap)  21.7 us
    pallas_call x2, Pallas kernels, run_gated(): pl.pallas_call(functools.partial(gated_kernel, offset, len(rows), tuple(s...  20.4 us
    ppermute x14, starting transfers between devices, beside(): return lax.ppermute(value, 'fs', col_swap)  12.9 us
    pallas_call x4, Pallas kernels, run_keep(): pl.pallas_call(functools.partial(keep_kernel, k), in_specs=[SMEM] + [VMEM...  10.5 us
    ppermute x12, starting transfers between devices, across(): return lax.ppermute(value, 'rep', swap)  10.3 us
  transfers between devices with their start and end apart: 77, of which 32 were waited for; matrix products, arithmetic and copies ran while one was open for 0% of the time, Pallas kernels for 16%

profile of v2, /device:TPU:0, one launch (start us, length us, event | category | flops | bytes accessed | tf_op | source)
XLA Modules:
  0.0 284.0 jit_solution(8363790524326260703)
XLA Ops:
  1.3 3.1 %collective-permute-start.6 = (bf16[2,128,512]{2,1,0:T(8,128)(2,1)S(1)}, bf16[2,128,512]{2,1,0:T(8,128)(2,1)S(1)}, u32[]{:S(2)}, u32[]{:S(2)}) collective-permute-start(bf16[2,128,512]{2,1,0:T(8,128)(2,1)S(1)} %fusion), channel_id=1, source_target_pairs={{0,4},{2,6},{4,8},{6,10},{8,12},{10,14},{12,0},{14,2},{1,5},{3,7},... | collective-permute-start | bytes 786440 | tf_op jit(solution)/shard_map/ppermute | solution.py:557
  16.0 4.8 %collective-permute-done.1 = f32[2,256]{1,0:T(2,128)S(1)} collective-permute-done((f32[2,256]{1,0:T(2,128)S(1)}, f32[2,256]{1,0:T(2,128)S(1)}, u32[]{:S(2)}, u32[]{:S(2)}) %collective-permute-start.1) | collective-permute-done | bytes 2080 | tf_op jit(solution)/shard_map/ppermute | solution.py:548
  22.3 4.5 %collective-permute-done.2.refs_6_.scale = f32[2,2,256]{2,1,0:T(2,128)S(1)} collective-permute-done((f32[2,2,256]{2,1,0:T(2,128)S(1)}, f32[2,2,256]{2,1,0:T(2,128)S(1)}, u32[]{:S(2)}, u32[]{:S(2)}) %collective-permute-start.2) | collective-permute-done | bytes 4128 | tf_op jit(solution)/shard_map/ppermute | solution.py:557
  27.2 5.0 %collective-permute-done.3.refs_7_.scale = f32[2,2,256]{2,1,0:T(2,128)S(1)} collective-permute-done((f32[2,2,256]{2,1,0:T(2,128)S(1)}, f32[2,2,256]{2,1,0:T(2,128)S(1)}, u32[]{:S(2)}, u32[]{:S(2)}) %collective-permute-start.3) | collective-permute-done | bytes 4128 | tf_op jit(solution)/shard_map/ppermute | solution.py:557
  32.2 5.4 %collective-permute-done.4.refs_8_.scale = f32[2,2,256]{2,1,0:T(2,128)S(1)} collective-permute-done((f32[2,2,256]{2,1,0:T(2,128)S(1)}, f32[2,2,256]{2,1,0:T(2,128)S(1)}, u32[]{:S(2)}, u32[]{:S(2)}) %collective-permute-start.4) | collective-permute-done | bytes 4128 | tf_op jit(solution)/shard_map/ppermute | solution.py:557
  45.3 4.2 %collective-permute-done.16.refs_21_ = bf16[2,128,512]{2,1,0:T(8,128)(2,1)S(1)} collective-permute-done((bf16[2,128,512]{2,1,0:T(8,128)(2,1)S(1)}, bf16[2,128,512]{2,1,0:T(8,128)(2,1)S(1)}, u32[]{:S(2)}, u32[]{:S(2)}) %collective-permute-start.16) | collective-permute-done | bytes 262176 | tf_op jit(solution)/shard_map/ppermute | solution.py:548
  57.4 7.9 %collective-permute-done.5.refs_10_ = bf16[2,256,512]{2,1,0:T(8,128)(2,1)S(1)} collective-permute-done((bf16[2,256,512]{2,1,0:T(8,128)(2,1)S(1)}, bf16[2,256,512]{2,1,0:T(8,128)(2,1)S(1)}, u32[]{:S(2)}, u32[]{:S(2)}) %collective-permute-start.5) | collective-permute-done | bytes 524320 | tf_op jit(solution)/shard_map/ppermute | solution.py:548
  66.2 4.3 %collective-permute-done.17.refs_22_ = bf16[2,128,512]{2,1,0:T(8,128)(2,1)S(1)} collective-permute-done((bf16[2,128,512]{2,1,0:T(8,128)(2,1)S(1)}, bf16[2,128,512]{2,1,0:T(8,128)(2,1)S(1)}, u32[]{:S(2)}, u32[]{:S(2)}) %collective-permute-start.17) | collective-permute-done | bytes 262176 | tf_op jit(solution)/shard_map/ppermute | solution.py:545
  70.5 4.8 %collective-permute-done.13.refs_18_ = bf16[2,128,512]{2,1,0:T(8,128)(2,1)S(1)} collective-permute-done((bf16[2,128,512]{2,1,0:T(8,128)(2,1)S(1)}, bf16[2,128,512]{2,1,0:T(8,128)(2,1)S(1)}, u32[]{:S(2)}, u32[]{:S(2)}) %collective-permute-start.13) | collective-permute-done | bytes 262176 | tf_op jit(solution)/shard_map/ppermute | solution.py:545
  76.1 4.6 %mixer.1 = (bf16[256,2048]{1,0:T(8,128)(2,1)S(1)}, bf16[256,2048]{1,0:T(8,128)(2,1)S(1)}) custom-call(s32[4]{0:T(128)S(1)} %pad_add_fusion.place.refs_0_, bf16[512,2048]{1,0:T(8,128)(2,1)S(1)} %get-tuple-element.39.refs_1_, f32[1,512]{1,0:T(1,128)S(1)} %bitcast.22, f32[128,512]{1,0:T(8,128)S(1)} %copy-done.4, f32[1,512]{1,0:T(1,128)S(1)} %bitcast.23, ...), custom_call_target="tpu_custom_call" | custom-call | flops 5000000000 | bytes 10000000 | tf_op jit(solution)/shard_map/mixer/pallas_call | solution.py:254
  81.3 3.6 %collective-permute-done.53 = bf16[704,256]{1,0:T(8,128)(2,1)S(1)} collective-permute-done((bf16[704,256]{1,0:T(8,128)(2,1)S(1)}, bf16[704,256]{1,0:T(8,128)(2,1)S(1)}, u32[]{:S(2)}, u32[]{:S(2)}) %collective-permute-start.53) | collective-permute-done | bytes 360480 | tf_op jit(solution)/shard_map/ppermute | solution.py:548
  85.9 11.4 %collective-permute-done.43.refs_10_ = bf16[256,640]{1,0:T(8,128)(2,1)S(1)} collective-permute-done((bf16[256,640]{1,0:T(8,128)(2,1)S(1)}, bf16[256,640]{1,0:T(8,128)(2,1)S(1)}, u32[]{:S(2)}, u32[]{:S(2)}) %collective-permute-start.43) | collective-permute-done | bytes 327712 | tf_op jit(solution)/shard_map/ppermute | solution.py:557
  97.3 7.0 %collective-permute-done.45.refs_12_ = bf16[256,640]{1,0:T(8,128)(2,1)S(1)} collective-permute-done((bf16[256,640]{1,0:T(8,128)(2,1)S(1)}, bf16[256,640]{1,0:T(8,128)(2,1)S(1)}, u32[]{:S(2)}, u32[]{:S(2)}) %collective-permute-start.45) | collective-permute-done | bytes 327712 | tf_op jit(solution)/shard_map/ppermute | solution.py:557
  104.9 8.0 %collective-permute-done.28.refs_14_ = bf16[256,768]{1,0:T(8,128)(2,1)S(1)} collective-permute-done((bf16[256,768]{1,0:T(8,128)(2,1)S(1)}, bf16[256,768]{1,0:T(8,128)(2,1)S(1)}, u32[]{:S(2)}, u32[]{:S(2)}) %collective-permute-start.28) | collective-permute-done | bytes 393248 | tf_op jit(solution)/shard_map/ppermute | solution.py:557
  114.4 6.9 %collective-permute-done.30.refs_16_ = bf16[256,768]{1,0:T(8,128)(2,1)S(1)} collective-permute-done((bf16[256,768]{1,0:T(8,128)(2,1)S(1)}, bf16[256,768]{1,0:T(8,128)(2,1)S(1)}, u32[]{:S(2)}, u32[]{:S(2)}) %collective-permute-start.30) | collective-permute-done | bytes 393248 | tf_op jit(solution)/shard_map/ppermute | solution.py:557
  121.3 14.3 %collective-permute-start.49 = (bf16[256,640]{1,0:T(8,128)(2,1)S(1)}, bf16[256,640]{1,0:T(8,128)(2,1)S(1)}, u32[]{:S(2)}, u32[]{:S(2)}) collective-permute-start(bf16[256,640]{1,0:T(8,128)(2,1)S(1)} %collective-permute-done.45.refs_12_), channel_id=1, source_target_pairs={{0,4},{2,6},{4,8},{6,10},{8,12},{10,14},{12,0},{14,2},{1,5},{3,7},... | collective-permute-start | bytes 983048 | tf_op jit(solution)/shard_map/ppermute | solution.py:557
  138.2 7.3 %collective-permute-done.47.refs_14_ = bf16[256,640]{1,0:T(8,128)(2,1)S(1)} collective-permute-done((bf16[256,640]{1,0:T(8,128)(2,1)S(1)}, bf16[256,640]{1,0:T(8,128)(2,1)S(1)}, u32[]{:S(2)}, u32[]{:S(2)}) %collective-permute-start.47) | collective-permute-done | bytes 327712 | tf_op jit(solution)/shard_map/ppermute | solution.py:557
  145.5 7.0 %collective-permute-done.49.refs_16_ = bf16[256,640]{1,0:T(8,128)(2,1)S(1)} collective-permute-done((bf16[256,640]{1,0:T(8,128)(2,1)S(1)}, bf16[256,640]{1,0:T(8,128)(2,1)S(1)}, u32[]{:S(2)}, u32[]{:S(2)}) %collective-permute-start.49) | collective-permute-done | bytes 327712 | tf_op jit(solution)/shard_map/ppermute | solution.py:557
  154.8 13.1 %collective-permute-done.54.refs_0_ = bf16[2,704,256]{2,1,0:T(8,128)(2,1)S(1)} collective-permute-done((bf16[2,704,256]{2,1,0:T(8,128)(2,1)S(1)}, bf16[2,704,256]{2,1,0:T(8,128)(2,1)S(1)}, u32[]{:S(2)}, u32[]{:S(2)}) %collective-permute-start.54) | collective-permute-done | bytes 720928 | tf_op jit(solution)/shard_map/ppermute | solution.py:557
  167.9 8.4 %collective-permute-done.32.refs_18_ = bf16[256,768]{1,0:T(8,128)(2,1)S(1)} collective-permute-done((bf16[256,768]{1,0:T(8,128)(2,1)S(1)}, bf16[256,768]{1,0:T(8,128)(2,1)S(1)}, u32[]{:S(2)}, u32[]{:S(2)}) %collective-permute-start.32) | collective-permute-done | bytes 393248 | tf_op jit(solution)/shard_map/ppermute | solution.py:557
  176.4 5.3 %collective-permute-done.34.refs_20_ = bf16[256,768]{1,0:T(8,128)(2,1)S(1)} collective-permute-done((bf16[256,768]{1,0:T(8,128)(2,1)S(1)}, bf16[256,768]{1,0:T(8,128)(2,1)S(1)}, u32[]{:S(2)}, u32[]{:S(2)}) %collective-permute-start.34) | collective-permute-done | bytes 393248 | tf_op jit(solution)/shard_map/ppermute | solution.py:557
  183.8 14.7 %collective-permute-done.51.refs_18_ = bf16[256,640]{1,0:T(8,128)(2,1)S(1)} collective-permute-done((bf16[256,640]{1,0:T(8,128)(2,1)S(1)}, bf16[256,640]{1,0:T(8,128)(2,1)S(1)}, u32[]{:S(2)}, u32[]{:S(2)}) %collective-permute-start.51) | collective-permute-done | bytes 327712 | tf_op jit(solution)/shard_map/ppermute | solution.py:557
  201.5 10.6 %gated.2 = (bf16[1024,768]{1,0:T(8,128)(2,1)S(1)}, bf16[1024,2048]{1,0:T(8,128)(2,1)S(1)}) custom-call(s32[4]{0:T(128)S(1)} %pad_add_fusion.place.refs_0_, f32[8,1408]{1,0:T(8,128)S(1)} %get-tuple-element.37.refs_1_, f32[8,1408]{1,0:T(8,128)S(1)} %collective-permute-done.refs_2_, bf16[256,2048]{1,0:T(8,128)(2,1)S(1)} %get-tuple-element.43.refs_3_, ...), custom_call_target="tpu_custom_call" | custom-call | flops 6000000000 | bytes 12000000 | tf_op jit(solution)/shard_map/gated/pallas_call | solution.py:410
  212.7 6.4 %collective-permute-done.55.refs_0_ = bf16[2,704,256]{2,1,0:T(8,128)(2,1)S(1)} collective-permute-done((bf16[2,704,256]{2,1,0:T(8,128)(2,1)S(1)}, bf16[2,704,256]{2,1,0:T(8,128)(2,1)S(1)}, u32[]{:S(2)}, u32[]{:S(2)}) %collective-permute-start.55) | collective-permute-done | bytes 720928 | tf_op jit(solution)/shard_map/ppermute | solution.py:557
  219.1 9.8 %gated.3.late = bf16[1024,640]{1,0:T(8,128)(2,1)S(1)} custom-call(s32[4]{0:T(128)S(1)} %pad_add_fusion.place.refs_0_, f32[8,1408]{1,0:T(8,128)S(1)} %get-tuple-element.37.refs_1_, f32[8,1408]{1,0:T(8,128)S(1)} %collective-permute-done.refs_2_, bf16[1024,2048]{1,0:T(8,128)(2,1)S(1)} %get-tuple-element.47.refs_3_, ...), custom_call_target="tpu_custom_call" | custom-call | flops 6000000000 | bytes 12000000 | tf_op jit(solution)/shard_map/gated/pallas_call | solution.py:410
  239.7 2.7 keep.5
  244.0 3.3 %collective-permute-done.74.second = bf16[256,512]{1,0:T(8,128)(2,1)S(1)} collective-permute-done((bf16[256,512]{1,0:T(8,128)(2,1)S(1)}, bf16[256,512]{1,0:T(8,128)(2,1)S(1)}, u32[]{:S(2)}, u32[]{:S(2)}) %collective-permute-start.74) | collective-permute-done | bytes 262176 | tf_op jit(solution)/shard_map/ppermute | solution.py:548
  248.9 3.2 %collective-permute-done.67.first = bf16[256,512]{1,0:T(8,128)(2,1)S(1)} collective-permute-done((bf16[256,512]{1,0:T(8,128)(2,1)S(1)}, bf16[256,512]{1,0:T(8,128)(2,1)S(1)}, u32[]{:S(2)}, u32[]{:S(2)}) %collective-permute-start.67) | collective-permute-done | bytes 262176 | tf_op jit(solution)/shard_map/ppermute | solution.py:545
  260.3 3.1 %collective-permute-done.62.first = bf16[256,512]{1,0:T(8,128)(2,1)S(1)} collective-permute-done((bf16[256,512]{1,0:T(8,128)(2,1)S(1)}, bf16[256,512]{1,0:T(8,128)(2,1)S(1)}, u32[]{:S(2)}, u32[]{:S(2)}) %collective-permute-start.62) | collective-permute-done | bytes 262176 | tf_op jit(solution)/shard_map/ppermute | solution.py:545
  264.8 5.0 %collective-permute-done.63.second = bf16[256,512]{1,0:T(8,128)(2,1)S(1)} collective-permute-done((bf16[256,512]{1,0:T(8,128)(2,1)S(1)}, bf16[256,512]{1,0:T(8,128)(2,1)S(1)}, u32[]{:S(2)}, u32[]{:S(2)}) %collective-permute-start.63) | collective-permute-done | bytes 262176 | tf_op jit(solution)/shard_map/ppermute | solution.py:548
  270.4 4.2 %collective-permute-done.57.first = bf16[256,512]{1,0:T(8,128)(2,1)S(1)} collective-permute-done((bf16[256,512]{1,0:T(8,128)(2,1)S(1)}, bf16[256,512]{1,0:T(8,128)(2,1)S(1)}, u32[]{:S(2)}, u32[]{:S(2)}) %collective-permute-start.57) | collective-permute-done | bytes 262176 | tf_op jit(solution)/shard_map/ppermute | solution.py:545
  274.6 5.8 %collective-permute-done.58.second = bf16[256,512]{1,0:T(8,128)(2,1)S(1)} collective-permute-done((bf16[256,512]{1,0:T(8,128)(2,1)S(1)}, bf16[256,512]{1,0:T(8,128)(2,1)S(1)}, u32[]{:S(2)}, u32[]{:S(2)}) %collective-permute-start.58) | collective-permute-done | bytes 262176 | tf_op jit(solution)/shard_map/ppermute | solution.py:548
  (176 shorter events, 73.7 us)
Async XLA Ops:
  10.0 31.1 %collective-permute-start.39 = (bf16[256,640]{1,0:T(8,128)(2,1)S(1)}, bf16[256,640]{1,0:T(8,128)(2,1)S(1)}, u32[]{:S(2)}, u32[]{:S(2)}) collective-permute-start(bf16[256,640]{1,0:T(8,128)(2,1)S(1)} %get-tuple-element.49), channel_id=1, source_target_pairs={{0,2},{2,0},{4,6},{6,4},{8,10},{10,8},{12,14},{14,12},{1,3},{3,1},... | collective-permute-start | bytes 983048 | tf_op jit(solution)/shard_map/ppermute | solution.py:548
  11.6 28.8 %collective-permute-start.14 = (bf16[2,128,512]{2,1,0:T(8,128)(2,1)S(1)}, bf16[2,128,512]{2,1,0:T(8,128)(2,1)S(1)}, u32[]{:S(2)}, u32[]{:S(2)}) collective-permute-start(bf16[2,128,512]{2,1,0:T(8,128)(2,1)S(1)} %fusion), channel_id=1, source_target_pairs={{0,12},{2,14},{4,0},{6,2},{8,4},{10,6},{12,8},{14,10},{1,13},{3,15... | collective-permute-start | bytes 786440 | tf_op jit(solution)/shard_map/ppermute | solution.py:557
  13.8 27.9 %collective-permute-start.10 = (bf16[2,128,512]{2,1,0:T(8,128)(2,1)S(1)}, bf16[2,128,512]{2,1,0:T(8,128)(2,1)S(1)}, u32[]{:S(2)}, u32[]{:S(2)}) collective-permute-start(bf16[2,128,512]{2,1,0:T(8,128)(2,1)S(1)} %collective-permute-done.6.refs_11_), channel_id=1, source_target_pairs={{0,4},{2,6},{4,8},{6,10},{8,12},{10,14},{12,0},{14,2},{1,5},{3,7},... | collective-permute-start | bytes 786440 | tf_op jit(solution)/shard_map/ppermute | solution.py:557
  14.4 28.6 %collective-permute-start.8 = (bf16[2,128,512]{2,1,0:T(8,128)(2,1)S(1)}, bf16[2,128,512]{2,1,0:T(8,128)(2,1)S(1)}, u32[]{:S(2)}, u32[]{:S(2)}) collective-permute-start(bf16[2,128,512]{2,1,0:T(8,128)(2,1)S(1)} %collective-permute-done.6.refs_11_), channel_id=1, source_target_pairs={{0,2},{2,0},{4,6},{6,4},{8,10},{10,8},{12,14},{14,12},{1,3},{3,1},... | collective-permute-start | bytes 786440 | tf_op jit(solution)/shard_map/ppermute | solution.py:548
  43.0 22.3 %collective-permute-start.5 = (bf16[2,256,512]{2,1,0:T(8,128)(2,1)S(1)}, bf16[2,256,512]{2,1,0:T(8,128)(2,1)S(1)}, u32[]{:S(2)}, u32[]{:S(2)}) collective-permute-start(bf16[2,256,512]{2,1,0:T(8,128)(2,1)S(1)} %pad_maximum_fusion.1.refs_9_), channel_id=1, source_target_pairs={{0,2},{2,0},{4,6},{6,4},{8,10},{10,8},{12,14},{14,12},{1,3},{3,1},... | collective-permute-start | bytes 1572872 | tf_op jit(solution)/shard_map/ppermute | solution.py:548
  55.1 20.2 %collective-permute-start.13 = (bf16[2,128,512]{2,1,0:T(8,128)(2,1)S(1)}, bf16[2,128,512]{2,1,0:T(8,128)(2,1)S(1)}, u32[]{:S(2)}, u32[]{:S(2)}) collective-permute-start(bf16[2,128,512]{2,1,0:T(8,128)(2,1)S(1)} %collective-permute-done.12.refs_17_), channel_id=1, source_target_pairs={{0,16},{16,0},{1,17},{17,1},{2,18},{18,2},{3,19},{19,3},{4,20},{20... | collective-permute-start | bytes 786440 | tf_op jit(solution)/shard_map/ppermute | solution.py:545
  65.3 19.6 %collective-permute-start.24 = (bf16[256,768]{1,0:T(8,128)(2,1)S(1)}, bf16[256,768]{1,0:T(8,128)(2,1)S(1)}, u32[]{:S(2)}, u32[]{:S(2)}) collective-permute-start(bf16[256,768]{1,0:T(8,128)(2,1)S(1)} %get-tuple-element.45), channel_id=1, source_target_pairs={{0,2},{2,0},{4,6},{6,4},{8,10},{10,8},{12,14},{14,12},{1,3},{3,1},... | collective-permute-start | bytes 1179656 | tf_op jit(solution)/shard_map/ppermute | solution.py:548
  80.7 40.5 %collective-permute-start.18 = (bf16[256,2048]{1,0:T(8,128)(2,1)S(1)}, bf16[256,2048]{1,0:T(8,128)(2,1)S(1)}, u32[]{:S(2)}, u32[]{:S(2)}) collective-permute-start(bf16[256,2048]{1,0:T(8,128)(2,1)S(1)} %get-tuple-element.41), channel_id=1, source_target_pairs={{0,1},{1,0},{2,3},{3,2},{4,5},{5,4},{6,7},{7,6},{8,9},{9,8},{10,11... | collective-permute-start | bytes 3145736 | tf_op jit(solution)/shard_map/ppermute | solution.py:554
  84.9 19.4 %collective-permute-start.45 = (bf16[256,640]{1,0:T(8,128)(2,1)S(1)}, bf16[256,640]{1,0:T(8,128)(2,1)S(1)}, u32[]{:S(2)}, u32[]{:S(2)}) collective-permute-start(bf16[256,640]{1,0:T(8,128)(2,1)S(1)} %collective-permute-done.41.refs_8_), channel_id=1, source_target_pairs={{0,4},{2,6},{4,8},{6,10},{8,12},{10,14},{12,0},{14,2},{1,5},{3,7},... | collective-permute-start | bytes 983048 | tf_op jit(solution)/shard_map/ppermute | solution.py:557
  85.4 18.9 %collective-permute-start.40 = (bf16[256,640]{1,0:T(8,128)(2,1)S(1)}, bf16[256,640]{1,0:T(8,128)(2,1)S(1)}, u32[]{:S(2)}, u32[]{:S(2)}) collective-permute-start(bf16[256,640]{1,0:T(8,128)(2,1)S(1)} %collective-permute-done.39.refs_6_), channel_id=1, source_target_pairs={{0,1},{1,0},{2,3},{3,2},{4,5},{5,4},{6,7},{7,6},{8,9},{9,8},{10,11... | collective-permute-start | bytes 983048 | tf_op jit(solution)/shard_map/ppermute | solution.py:554
  85.4 18.9 %collective-permute-start.42 = (bf16[256,640]{1,0:T(8,128)(2,1)S(1)}, bf16[256,640]{1,0:T(8,128)(2,1)S(1)}, u32[]{:S(2)}, u32[]{:S(2)}) collective-permute-start(bf16[256,640]{1,0:T(8,128)(2,1)S(1)} %collective-permute-done.41.refs_8_), channel_id=1, source_target_pairs={{0,1},{1,0},{2,3},{3,2},{4,5},{5,4},{6,7},{7,6},{8,9},{9,8},{10,11... | collective-permute-start | bytes 983048 | tf_op jit(solution)/shard_map/ppermute | solution.py:554
  104.3 32.9 %collective-permute-start.27 = (bf16[256,768]{1,0:T(8,128)(2,1)S(1)}, bf16[256,768]{1,0:T(8,128)(2,1)S(1)}, u32[]{:S(2)}, u32[]{:S(2)}) collective-permute-start(bf16[256,768]{1,0:T(8,128)(2,1)S(1)} %collective-permute-done.26.refs_12_), channel_id=1, source_target_pairs={{0,1},{1,0},{2,3},{3,2},{4,5},{5,4},{6,7},{7,6},{8,9},{9,8},{10,11... | collective-permute-start | bytes 1179656 | tf_op jit(solution)/shard_map/ppermute | solution.py:554
  112.9 41.2 %collective-permute-start.71 = (bf16[2,704,256]{2,1,0:T(8,128)(2,1)S(1)}, bf16[2,704,256]{2,1,0:T(8,128)(2,1)S(1)}, u32[]{:S(2)}, u32[]{:S(2)}) collective-permute-start(bf16[2,704,256]{2,1,0:T(8,128)(2,1)S(1)} %pad_maximum_fusion.refs_0_), channel_id=1, source_target_pairs={{0,12},{2,14},{4,0},{6,2},{8,4},{10,6},{12,8},{14,10},{1,13},{3,15... | collective-permute-start | bytes 2162696 | tf_op jit(solution)/shard_map/ppermute | solution.py:557
  121.3 24.2 %collective-permute-start.47 = (bf16[256,640]{1,0:T(8,128)(2,1)S(1)}, bf16[256,640]{1,0:T(8,128)(2,1)S(1)}, u32[]{:S(2)}, u32[]{:S(2)}) collective-permute-start(bf16[256,640]{1,0:T(8,128)(2,1)S(1)} %collective-permute-done.43.refs_10_), channel_id=1, source_target_pairs={{0,4},{2,6},{4,8},{6,10},{8,12},{10,14},{12,0},{14,2},{1,5},{3,7},... | collective-permute-start | bytes 983048 | tf_op jit(solution)/shard_map/ppermute | solution.py:557
  121.3 31.2 %collective-permute-start.44 = (bf16[256,640]{1,0:T(8,128)(2,1)S(1)}, bf16[256,640]{1,0:T(8,128)(2,1)S(1)}, u32[]{:S(2)}, u32[]{:S(2)}) collective-permute-start(bf16[256,640]{1,0:T(8,128)(2,1)S(1)} %collective-permute-done.43.refs_10_), channel_id=1, source_target_pairs={{0,1},{1,0},{2,3},{3,2},{4,5},{5,4},{6,7},{7,6},{8,9},{9,8},{10,11... | collective-permute-start | bytes 983048 | tf_op jit(solution)/shard_map/ppermute | solution.py:554
  121.3 31.2 %collective-permute-start.49 = (bf16[256,640]{1,0:T(8,128)(2,1)S(1)}, bf16[256,640]{1,0:T(8,128)(2,1)S(1)}, u32[]{:S(2)}, u32[]{:S(2)}) collective-permute-start(bf16[256,640]{1,0:T(8,128)(2,1)S(1)} %collective-permute-done.45.refs_12_), channel_id=1, source_target_pairs={{0,4},{2,6},{4,8},{6,10},{8,12},{10,14},{12,0},{14,2},{1,5},{3,7},... | collective-permute-start | bytes 983048 | tf_op jit(solution)/shard_map/ppermute | solution.py:557
  137.3 44.4 %collective-permute-start.20 = (bf16[256,2048]{1,0:T(8,128)(2,1)S(1)}, bf16[256,2048]{1,0:T(8,128)(2,1)S(1)}, u32[]{:S(2)}, u32[]{:S(2)}) collective-permute-start(bf16[256,2048]{1,0:T(8,128)(2,1)S(1)} %get-tuple-element.43.refs_3_), channel_id=1, source_target_pairs={{0,2},{2,0},{4,6},{6,4},{8,10},{10,8},{12,14},{14,12},{1,3},{3,1},... | collective-permute-start | bytes 3145736 | tf_op jit(solution)/shard_map/ppermute | solution.py:548
  145.4 22.5 %collective-permute-start.54 = (bf16[2,704,256]{2,1,0:T(8,128)(2,1)S(1)}, bf16[2,704,256]{2,1,0:T(8,128)(2,1)S(1)}, u32[]{:S(2)}, u32[]{:S(2)}) collective-permute-start(bf16[2,704,256]{2,1,0:T(8,128)(2,1)S(1)} %pad_maximum_fusion.refs_0_), channel_id=1, source_target_pairs={{0,4},{2,6},{4,8},{6,10},{8,12},{10,14},{12,0},{14,2},{1,5},{3,7},... | collective-permute-start | bytes 2162696 | tf_op jit(solution)/shard_map/ppermute | solution.py:557
  152.5 30.3 %collective-permute-start.19 = (bf16[256,2048]{1,0:T(8,128)(2,1)S(1)}, bf16[256,2048]{1,0:T(8,128)(2,1)S(1)}, u32[]{:S(2)}, u32[]{:S(2)}) collective-permute-start(bf16[256,2048]{1,0:T(8,128)(2,1)S(1)} %get-tuple-element.43.refs_3_), channel_id=1, source_target_pairs={{0,16},{16,0},{1,17},{17,1},{2,18},{18,2},{3,19},{19,3},{4,20},{20... | collective-permute-start | bytes 3145736 | tf_op jit(solution)/shard_map/ppermute | solution.py:545
  154.1 22.2 %collective-permute-start.32 = (bf16[256,768]{1,0:T(8,128)(2,1)S(1)}, bf16[256,768]{1,0:T(8,128)(2,1)S(1)}, u32[]{:S(2)}, u32[]{:S(2)}) collective-permute-start(bf16[256,768]{1,0:T(8,128)(2,1)S(1)} %collective-permute-done.28.refs_14_), channel_id=1, source_target_pairs={{0,4},{2,6},{4,8},{6,10},{8,12},{10,14},{12,0},{14,2},{1,5},{3,7},... | collective-permute-start | bytes 1179656 | tf_op jit(solution)/shard_map/ppermute | solution.py:557
  154.1 27.6 %collective-permute-start.34 = (bf16[256,768]{1,0:T(8,128)(2,1)S(1)}, bf16[256,768]{1,0:T(8,128)(2,1)S(1)}, u32[]{:S(2)}, u32[]{:S(2)}) collective-permute-start(bf16[256,768]{1,0:T(8,128)(2,1)S(1)} %collective-permute-done.30.refs_16_), channel_id=1, source_target_pairs={{0,4},{2,6},{4,8},{6,10},{8,12},{10,14},{12,0},{14,2},{1,5},{3,7},... | collective-permute-start | bytes 1179656 | tf_op jit(solution)/shard_map/ppermute | solution.py:557
  182.8 18.1 %collective-permute-start.21 = (bf16[128,2048]{1,0:T(8,128)(2,1)S(1)}, bf16[128,2048]{1,0:T(8,128)(2,1)S(1)}, u32[]{:S(2)}, u32[]{:S(2)}) collective-permute-start(bf16[128,2048]{1,0:T(8,128)(2,1)S(1)} %slice.8), channel_id=1, source_target_pairs={{0,16},{16,0},{1,17},{17,1},{2,18},{18,2},{3,19},{19,3},{4,20},{20... | collective-permute-start | bytes 1572872 | tf_op jit(solution)/shard_map/ppermute | solution.py:545
  182.9 18.4 %collective-permute-start.22 = (bf16[128,2048]{1,0:T(8,128)(2,1)S(1)}, bf16[128,2048]{1,0:T(8,128)(2,1)S(1)}, u32[]{:S(2)}, u32[]{:S(2)}) collective-permute-start(bf16[128,2048]{1,0:T(8,128)(2,1)S(1)} %slice.9), channel_id=1, source_target_pairs={{0,2},{2,0},{4,6},{6,4},{8,10},{10,8},{12,14},{14,12},{1,3},{3,1},... | collective-permute-start | bytes 1572872 | tf_op jit(solution)/shard_map/ppermute | solution.py:548
  199.1 20.1 %collective-permute-start.55 = (bf16[2,704,256]{2,1,0:T(8,128)(2,1)S(1)}, bf16[2,704,256]{2,1,0:T(8,128)(2,1)S(1)}, u32[]{:S(2)}, u32[]{:S(2)}) collective-permute-start(bf16[2,704,256]{2,1,0:T(8,128)(2,1)S(1)} %collective-permute-done.54.refs_0_), channel_id=1, source_target_pairs={{0,4},{2,6},{4,8},{6,10},{8,12},{10,14},{12,0},{14,2},{1,5},{3,7},... | collective-permute-start | bytes 2162696 | tf_op jit(solution)/shard_map/ppermute | solution.py:557
  201.0 28.0 %collective-permute-start.72 = (bf16[2,704,256]{2,1,0:T(8,128)(2,1)S(1)}, bf16[2,704,256]{2,1,0:T(8,128)(2,1)S(1)}, u32[]{:S(2)}, u32[]{:S(2)}) collective-permute-start(bf16[2,704,256]{2,1,0:T(8,128)(2,1)S(1)} %collective-permute-done.71.refs_0_), channel_id=1, source_target_pairs={{0,1},{1,0},{2,3},{3,2},{4,5},{5,4},{6,7},{7,6},{8,9},{9,8},{10,11... | collective-permute-start | bytes 2162696 | tf_op jit(solution)/shard_map/ppermute | solution.py:554
  201.3 17.8 %collective-permute-start.52 = (bf16[256,640]{1,0:T(8,128)(2,1)S(1)}, bf16[256,640]{1,0:T(8,128)(2,1)S(1)}, u32[]{:S(2)}, u32[]{:S(2)}) collective-permute-start(bf16[256,640]{1,0:T(8,128)(2,1)S(1)} %collective-permute-done.51.refs_18_), channel_id=1, source_target_pairs={{0,1},{1,0},{2,3},{3,2},{4,5},{5,4},{6,7},{7,6},{8,9},{9,8},{10,11... | collective-permute-start | bytes 983048 | tf_op jit(solution)/shard_map/ppermute | solution.py:554
  212.1 25.6 %collective-permute-start.61 = (bf16[2,704,256]{2,1,0:T(8,128)(2,1)S(1)}, bf16[2,704,256]{2,1,0:T(8,128)(2,1)S(1)}, u32[]{:S(2)}, u32[]{:S(2)}) collective-permute-start(bf16[2,704,256]{2,1,0:T(8,128)(2,1)S(1)} %pad_maximum_fusion.refs_0_), channel_id=1, source_target_pairs={{0,1},{1,0},{2,3},{3,2},{4,5},{5,4},{6,7},{7,6},{8,9},{9,8},{10,11... | collective-permute-start | bytes 2162696 | tf_op jit(solution)/shard_map/ppermute | solution.py:554
  212.6 20.9 %collective-permute-start.66 = (bf16[2,704,256]{2,1,0:T(8,128)(2,1)S(1)}, bf16[2,704,256]{2,1,0:T(8,128)(2,1)S(1)}, u32[]{:S(2)}, u32[]{:S(2)}) collective-permute-start(bf16[2,704,256]{2,1,0:T(8,128)(2,1)S(1)} %collective-permute-done.54.refs_0_), channel_id=1, source_target_pairs={{0,1},{1,0},{2,3},{3,2},{4,5},{5,4},{6,7},{7,6},{8,9},{9,8},{10,11... | collective-permute-start | bytes 2162696 | tf_op jit(solution)/shard_map/ppermute | solution.py:554
  219.1 19.7 %collective-permute-start.56 = (bf16[2,704,256]{2,1,0:T(8,128)(2,1)S(1)}, bf16[2,704,256]{2,1,0:T(8,128)(2,1)S(1)}, u32[]{:S(2)}, u32[]{:S(2)}) collective-permute-start(bf16[2,704,256]{2,1,0:T(8,128)(2,1)S(1)} %collective-permute-done.55.refs_0_), channel_id=1, source_target_pairs={{0,1},{1,0},{2,3},{3,2},{4,5},{5,4},{6,7},{7,6},{8,9},{9,8},{10,11... | collective-permute-start | bytes 2162696 | tf_op jit(solution)/shard_map/ppermute | solution.py:554
  238.9 19.7 %collective-permute-start.68 = (bf16[256,512]{1,0:T(8,128)(2,1)S(1)}, bf16[256,512]{1,0:T(8,128)(2,1)S(1)}, u32[]{:S(2)}, u32[]{:S(2)}) collective-permute-start(bf16[256,512]{1,0:T(8,128)(2,1)S(1)} %get-tuple-element.63), channel_id=1, source_target_pairs={{0,2},{2,0},{4,6},{6,4},{8,10},{10,8},{12,14},{14,12},{1,3},{3,1},... | collective-permute-start | bytes 786440 | tf_op jit(solution)/shard_map/ppermute | solution.py:548
  248.3 21.5 %collective-permute-start.63 = (bf16[256,512]{1,0:T(8,128)(2,1)S(1)}, bf16[256,512]{1,0:T(8,128)(2,1)S(1)}, u32[]{:S(2)}, u32[]{:S(2)}) collective-permute-start(bf16[256,512]{1,0:T(8,128)(2,1)S(1)} %get-tuple-element.59), channel_id=1, source_target_pairs={{0,2},{2,0},{4,6},{6,4},{8,10},{10,8},{12,14},{14,12},{1,3},{3,1},... | collective-permute-start | bytes 786440 | tf_op jit(solution)/shard_map/ppermute | solution.py:548
  259.7 20.7 %collective-permute-start.58 = (bf16[256,512]{1,0:T(8,128)(2,1)S(1)}, bf16[256,512]{1,0:T(8,128)(2,1)S(1)}, u32[]{:S(2)}, u32[]{:S(2)}) collective-permute-start(bf16[256,512]{1,0:T(8,128)(2,1)S(1)} %get-tuple-element.55), channel_id=1, source_target_pairs={{0,2},{2,0},{4,6},{6,4},{8,10},{10,8},{12,14},{14,12},{1,3},{3,1},... | collective-permute-start | bytes 786440 | tf_op jit(solution)/shard_map/ppermute | solution.py:548
  (58 other events, 681.7 us)
